TPU v7x, 256 devices: a 4x2x16 block of a 4x16x16 slice. The times are simulated.
256 devices in a mesh: grp: 2 (over y), sp: 32 (over z, core), tp: 4 (over x).
Axes of the slice: x: 4, y: 2, z: 16, core: 2. Of those that a mesh axis runs over, the one named last changes fastest.
The devices are a block of a 4x16x16 slice.
Arguments:
- latent: bfloat16 [16384, 512], P(('grp', 'sp')), parts along dimension 0, may hold values from -6 to 6
- rope_key: bfloat16 [16384, 64], P(('grp', 'sp')), parts along dimension 0, may hold values from -6 to 6
- wide_query: bfloat16 [16384, 1536], P(('grp', 'sp'), 'tp'), parts along dimension 0, may hold values from -1300 to 1300
- narrow_query: bfloat16 [16384, 1024], P(('grp', 'sp'), 'tp'), parts along dimension 0, may hold values from -1300 to 1300
- wide_key_weight: bfloat16 [512, 1024], P(None, 'tp'), may hold values from -0.25 to 0.25
- wide_value_weight: bfloat16 [512, 1024], P(None, 'tp'), may hold values from -0.25 to 0.25
- narrow_key_weight: bfloat16 [512, 512], P(None, 'tp'), may hold values from -0.25 to 0.25
- narrow_value_weight: bfloat16 [512, 512], P(None, 'tp'), may hold values from -0.25 to 0.25
- latent_norm_scale: float32 [512], replicated, may hold values from 0.1 to 1.9
- out_wide: bfloat16 [1024, 4096], P('tp'), may hold values from -0.4375 to 0.4375
- out_narrow: bfloat16 [512, 4096], P('tp'), may hold values from -0.4375 to 0.4375
- residual: bfloat16 [16384, 4096], P(('grp', 'sp', 'tp')), parts along dimension 0, may hold values from -6 to 6
- ffn_gain: float32 [4096], replicated, may hold values from 0.1 to 1.9
- shared_gate: bfloat16 [4096, 512], P(None, 'tp'), may hold values from -0.09375 to 0.09375
- shared_up: bfloat16 [4096, 512], P(None, 'tp'), may hold values from -0.09375 to 0.09375
- shared_down: bfloat16 [512, 4096], P('tp'), may hold values from -0.25 to 0.25
- expert_gate: bfloat16 [128, 4096, 192], P(('sp', 'tp')), may hold values from -0.09375 to 0.09375
- expert_up: bfloat16 [128, 4096, 192], P(('sp', 'tp')), may hold values from -0.09375 to 0.09375
- expert_down: bfloat16 [128, 192, 4096], P(('sp', 'tp')), may hold values from -0.4375 to 0.4375
- routes: int32 [16384, 2], P(('grp', 'sp', 'tp')), parts along dimension 0, may hold values from 0 to 127, all different within a row; in each aligned block of 64 rows (0 to 63, 64 to 127, ...) at most 2 rows name the same one
- route_weights: float32 [16384, 2], P(('grp', 'sp', 'tp')), parts along dimension 0, may hold values from 0.25 to 1.5
Outputs:
- layer_out: bfloat16 [16384, 4096], P(('grp', 'sp', 'tp')), parts along dimension 0
There are 2 independent parts, one for each index of `grp`. A program takes and returns all parts, laid end to end along the dimension named above; an argument that names none is the same for every part. Nothing has to cross between parts.
Inputs may be any that keep to these rules, and one draw needn't show every extreme that they name: `routes`: each row names 2 different experts; in each aligned block of 64 rows no expert is named by more than 2 rows, and some block has an expert named exactly 2 times.
All inputs are finite; a program needn't handle non-finite values.
Results may differ from a plain program's by a relative error of at most 0.023.
Values may be sent and summed in bfloat16 or wider, within the bound.
A program may use at most 128 MiB of HBM per device.

v0:
```python
import math

import jax
import jax.numpy as jnp
from jax import lax
from jax.sharding import PartitionSpec as P

ROPE = 64
WIDE_HEAD_SIZE = 128
NARROW_HEAD_SIZE = 64


EPS = 1e-06
ROPE_BASE = 10000.0
NEG_FILL = -1e30


def sent_together(arrays, axis, dim, along):
    both = jnp.concatenate(arrays, axis=along)
    whole, at, outs = (lax.all_gather(both, axis, axis=dim, tiled=True), 0, [])
    for a in arrays:
        outs.append(lax.slice_in_dim(whole, at, at + a.shape[along], axis=along))
        at += a.shape[along]
    return tuple(outs)


def split_up(array, dim, peers):
    before, after = (array.shape[:dim], array.shape[dim + 1 :])
    return jnp.moveaxis(array.reshape(*before, peers, -1, *after), dim, 0)


def summed_on_arrival(array, axis, dim):
    peers = lax.axis_size(axis)
    blocks = lax.all_to_all(split_up(array, dim, peers), axis, 0, 0, tiled=True)
    return jnp.sum(blocks.astype(jnp.float32), axis=0)


def rotate(values, positions):
    half_size = values.shape[-1] // 2
    inverse = ROPE_BASE ** (-jnp.arange(half_size, dtype=jnp.float32) * 2.0 / values.shape[-1])
    angles = positions.astype(jnp.float32)[:, None] * inverse[None, :]
    shaped = (angles.shape[0],) + (1,) * (values.ndim - 2) + (half_size,)
    cosine_table = jnp.cos(angles).reshape(shaped)
    sine_table = jnp.sin(angles).reshape(shaped)
    first_half = values[..., :half_size]
    second_half = values[..., half_size:]
    return jnp.concatenate(
        [
            first_half * cosine_table - second_half * sine_table,
            second_half * cosine_table + first_half * sine_table,
        ],
        axis=-1,
    )


def rms_scale(values, gain):
    return values * lax.rsqrt(jnp.mean(values * values, axis=-1, keepdims=True) + EPS) * gain


def update(state, query_plain, query_turned, keys, turned_rows, values, visible, factor):
    running_max, running_sum, weighted = state
    scores = jnp.einsum("qhd,khd->hqk", query_plain, keys, preferred_element_type=jnp.float32)
    scores = scores + jnp.einsum(
        "qhr,kr->hqk", query_turned, turned_rows, preferred_element_type=jnp.float32
    )
    scores = jnp.where(visible[None], scores * factor, NEG_FILL)
    new_max = jnp.maximum(running_max, jnp.max(scores, axis=2))
    probs = jnp.where(visible[None], jnp.exp(scores - new_max[:, :, None]), 0.0)
    fading = jnp.exp(running_max - new_max)
    running_sum = running_sum * fading + jnp.sum(probs, axis=2)
    weighted = weighted * fading[:, :, None] + jnp.einsum(
        "hqk,khd->hqd", probs.astype(jnp.bfloat16), values, preferred_element_type=jnp.float32
    )
    return (new_max, running_sum, weighted)


def empty_state(heads, queries, value_size):
    return (
        jnp.full((heads, queries), NEG_FILL, jnp.float32),
        jnp.zeros((heads, queries), jnp.float32),
        jnp.zeros((heads, queries, value_size), jnp.float32),
    )


def finish(state):
    normal_sampler = state[2] / state[1][:, :, None]
    heads, queries, value_size = normal_sampler.shape
    return (
        normal_sampler.astype(jnp.bfloat16).transpose(1, 0, 2).reshape(queries, heads * value_size)
    )


def body(
    latent,
    rope_key,
    wide_query,
    narrow_query,
    wide_key_weight,
    wide_value_weight,
    narrow_key_weight,
    narrow_value_weight,
    latent_norm_scale,
    out_wide,
    out_narrow,
    residual,
    ffn_gain,
    shared_gate,
    shared_up,
    shared_down,
    expert_gate,
    expert_up,
    expert_down,
    routes,
    route_weights,
):
    tok_dev = latent.shape[0]
    seq_index = lax.axis_index("sp")
    own_pos = seq_index * tok_dev + jnp.arange(tok_dev, dtype=jnp.int32)
    last_pos = seq_index * tok_dev + tok_dev - 1
    normed_latent = rms_scale(latent.astype(jnp.float32), latent_norm_scale).astype(jnp.bfloat16)
    turned_key = rotate(rope_key.astype(jnp.float32), own_pos).astype(jnp.bfloat16)
    wide_heads_q = wide_query.reshape(tok_dev, -1, WIDE_HEAD_SIZE + ROPE)
    wide_plain = wide_heads_q[..., :WIDE_HEAD_SIZE]
    wide_turned = rotate(wide_heads_q[..., WIDE_HEAD_SIZE:].astype(jnp.float32), own_pos).astype(
        jnp.bfloat16
    )
    narrow_heads_q = narrow_query.reshape(tok_dev, -1, NARROW_HEAD_SIZE + ROPE)
    narrow_plain = narrow_heads_q[..., :NARROW_HEAD_SIZE]
    narrow_turned = rotate(
        narrow_heads_q[..., NARROW_HEAD_SIZE:].astype(jnp.float32), own_pos
    ).astype(jnp.bfloat16)
    wide_local = wide_plain.shape[1]
    narrow_local = narrow_plain.shape[1]
    wide_factor = (WIDE_HEAD_SIZE + ROPE) ** (-0.5)
    narrow_factor = (NARROW_HEAD_SIZE + ROPE) ** (-0.5)
    initial = empty_state(wide_local, tok_dev, WIDE_HEAD_SIZE) + empty_state(
        narrow_local, tok_dev, NARROW_HEAD_SIZE
    )
    pieces = sent_together((normed_latent, turned_key), "sp", 0, 1)
    indices = jnp.arange(pieces[0].shape[0], dtype=jnp.int32)
    placing = lambda positions: positions
    latent_rows, turned_rows = pieces
    length_rows = latent_rows.shape[0]
    block = math.gcd(length_rows, 512)

    def one_block(block_index, inner):
        lat_block = lax.dynamic_slice_in_dim(latent_rows, block_index * block, block, 0)
        turned_block = lax.dynamic_slice_in_dim(turned_rows, block_index * block, block, 0)
        key_pos = placing(lax.dynamic_slice_in_dim(indices, block_index * block, block, 0))

        def work(current):
            visible = key_pos[None, :] <= own_pos[:, None]
            wide_keys = (
                jnp.dot(lat_block, wide_key_weight, preferred_element_type=jnp.float32)
                .astype(jnp.bfloat16)
                .reshape(block, wide_local, WIDE_HEAD_SIZE)
            )
            wide_values = (
                jnp.dot(lat_block, wide_value_weight, preferred_element_type=jnp.float32)
                .astype(jnp.bfloat16)
                .reshape(block, wide_local, WIDE_HEAD_SIZE)
            )
            narrow_keys = (
                jnp.dot(lat_block, narrow_key_weight, preferred_element_type=jnp.float32)
                .astype(jnp.bfloat16)
                .reshape(block, narrow_local, NARROW_HEAD_SIZE)
            )
            narrow_values = (
                jnp.dot(lat_block, narrow_value_weight, preferred_element_type=jnp.float32)
                .astype(jnp.bfloat16)
                .reshape(block, narrow_local, NARROW_HEAD_SIZE)
            )
            wide_state = update(
                current[:3],
                wide_plain,
                wide_turned,
                wide_keys,
                turned_block,
                wide_values,
                visible,
                wide_factor,
            )
            narrow_state = update(
                current[3:],
                narrow_plain,
                narrow_turned,
                narrow_keys,
                turned_block,
                narrow_values,
                visible,
                narrow_factor,
            )
            return wide_state + narrow_state

        return lax.cond(jnp.min(key_pos) <= last_pos, work, lambda current: current, inner)

    final = lax.fori_loop(0, length_rows // block, one_block, initial)
    wide_mix = finish(final[:3])
    narrow_mix = finish(final[3:])
    projected = summed_on_arrival(
        (
            jnp.dot(wide_mix, out_wide, preferred_element_type=jnp.float32)
            + jnp.dot(narrow_mix, out_narrow, preferred_element_type=jnp.float32)
        ).astype(jnp.bfloat16),
        "tp",
        0,
    )
    stream = (residual.astype(jnp.float32) + projected).astype(jnp.bfloat16)
    normed = rms_scale(stream.astype(jnp.float32), ffn_gain).astype(jnp.bfloat16)
    piece = lax.all_gather(normed, "tp", axis=0, tiled=True)
    gate_part = jnp.dot(piece, shared_gate, preferred_element_type=jnp.float32)
    up_part = jnp.dot(piece, shared_up, preferred_element_type=jnp.float32)
    active = (jax.nn.silu(gate_part) * up_part).astype(jnp.bfloat16)
    shared_terms = jnp.dot(active, shared_down, preferred_element_type=jnp.float32)
    shared = lax.psum_scatter(
        shared_terms.astype(jnp.bfloat16), "tp", scatter_dimension=0, tiled=True
    ).astype(jnp.float32)
    rows_here, top_count = routes.shape
    local_experts = expert_gate.shape[0]
    experts_all = local_experts * lax.axis_size(("sp", "tp"))
    capacity = max(2, 2 * top_count * rows_here // experts_all)
    model_width = normed.shape[1]
    flat_routes = routes.reshape(-1)
    assigned = flat_routes.shape[0]
    choose = (flat_routes[:, None] == jnp.arange(experts_all, dtype=jnp.int32)[None, :]).astype(
        jnp.float32
    )
    lower_mask = (jnp.arange(assigned)[:, None] > jnp.arange(assigned)[None, :]).astype(jnp.float32)
    earlier = jnp.dot(lower_mask, choose, precision=lax.Precision.HIGHEST)
    slots = jnp.sum(earlier * choose, axis=1).astype(jnp.int32)
    target = flat_routes * capacity + slots
    send_map = jnp.any(
        target.reshape(rows_here, top_count)[None, :, :]
        == jnp.arange(experts_all * capacity, dtype=jnp.int32)[:, None, None],
        axis=2,
    ).astype(jnp.bfloat16)
    outgoing = jnp.dot(send_map, normed, preferred_element_type=jnp.float32).astype(jnp.bfloat16)
    outgoing = outgoing.reshape(experts_all, capacity, model_width)
    incoming = lax.all_to_all(outgoing, ("sp", "tp"), split_axis=0, concat_axis=0, tiled=True)
    sources = incoming.shape[0] // local_experts
    grouped = incoming.reshape(sources, local_experts, incoming.shape[1], model_width)
    gate_part = jnp.einsum(
        "sxcd,xdf->sxcf", grouped, expert_gate, preferred_element_type=jnp.float32
    )
    up_part = jnp.einsum("sxcd,xdf->sxcf", grouped, expert_up, preferred_element_type=jnp.float32)
    active = (jax.nn.silu(gate_part) * up_part).astype(jnp.bfloat16)
    finished = jnp.einsum(
        "sxcf,xfd->sxcd", active, expert_down, preferred_element_type=jnp.float32
    ).astype(jnp.bfloat16)
    returned = lax.all_to_all(
        finished.reshape(incoming.shape), ("sp", "tp"), split_axis=0, concat_axis=0, tiled=True
    )
    picked = returned.reshape(experts_all * capacity, model_width)[target]
    routed = jnp.sum(
        picked.reshape(rows_here, top_count, model_width).astype(jnp.float32)
        * route_weights[:, :, None],
        axis=1,
    )
    return (stream.astype(jnp.float32) + shared + routed).astype(jnp.bfloat16)


def solution(mesh):
    placed = (
        P(("grp", "sp"), None),
        P(("grp", "sp"), None),
        P(("grp", "sp"), "tp"),
        P(("grp", "sp"), "tp"),
        P(None, "tp"),
        P(None, "tp"),
        P(None, "tp"),
        P(None, "tp"),
        P(),
        P("tp", None),
        P("tp", None),
        P(("grp", "sp", "tp"), None),
        P(),
        P(None, "tp"),
        P(None, "tp"),
        P("tp", None),
        P(("sp", "tp"), None, None),
        P(("sp", "tp"), None, None),
        P(("sp", "tp"), None, None),
        P(("grp", "sp", "tp"), None),
        P(("grp", "sp", "tp"), None),
    )
    return jax.shard_map(
        body, mesh=mesh, in_specs=placed, out_specs=P(("grp", "sp", "tp"), None), check_vma=False
    )
```

profile of v0, /device:TPU:35, one launch (start us, length us, event | category | flops | bytes accessed | tf_op | source)
XLA Modules:
  0.0 665.9 jit_solution(9544668494291410742)
XLA Ops:
  11.7 111.4 %all-gather.3.cloned.1.call-done = bf16[8192,576]{0,1:T(8,128)(2,1)} async-done(((bf16[256,576]{0,1:T(8,128)(2,1)}), bf16[8192,576]{0,1:T(8,128)(2,1)}) %all-gather.3.cloned.1.call-update) | async-done | bytes 9437200 | tf_op jit(solution)/shard_map/all_gather | solution.py:20
  123.1 7.7 %slice.52 = bf16[8192,512]{0,1:T(8,128)(2,1)} slice(bf16[8192,576]{0,1:T(8,128)(2,1)} %all-gather.3.cloned.1.call-done), slice={[0:8192], [0:512]} | slice | bytes 16777216 | tf_op jit(solution)/shard_map/slice | solution.py:22
  130.8 11.9 %copy.73 = bf16[8192,512]{1,0:T(8,128)(2,1)} copy(bf16[8192,512]{0,1:T(8,128)(2,1)} %slice.52) | data formatting | bytes 16777216
  142.7 2.4 slice.54
  146.4 55.1 %while.24 = (s32[]{:T(128)}, f32[2,256]{1,0:T(2,128)S(1)}, f32[2,256]{1,0:T(2,128)}, f32[2,256,128]{2,1,0:T(8,128)S(1)}, f32[2,256]{1,0:T(2,128)S(1)}, /*index=5...) while((s32[]{:T(128)}, f32[2,256]{1,0:T(2,128)S(1)}, ...), condition=%wide.region_9.10_spmd.clone, body=%wide.region_1.9_spmd.clone.sunk | while | flops 677055232 | bytes 17331832 | solution.py:197
  147.0 1.5 fusion.130
  149.1 10.9 %conditional.3 = ((f32[2,256]{1,0:T(2,128)S(1)}, f32[2,256]{1,0:T(2,128)}, f32[2,256,128]{2,1,0:T(8,128)S(1)}, f32[2,256]{1,0:T(2,128)S(1)}, f32[2,256]{1,0:T(2,128)S(1)}, /*index=5*/f32[2,256,64]{1,2,0:T(8,128)S(1)})) conditional(s32[]{:T(128)} %convert_element_type.225, (f32[2,256]{1,0:T(2,128)S(1)}, f32[2,256]{1,0:T(2,128)}, ...), branch_computations={%region_3.0_spmd, %region_4.8_spmd} | conditional | flops 677054720 | bytes 17326224 | solution.py:195
  160.6 1.5 fusion.130
  163.4 1.5 fusion.130
  166.2 1.5 fusion.130
  168.9 1.5 fusion.130
  202.3 2.0 fusion.104
  204.3 2.1 fusion.36
  206.4 4.8 all-to-all-start
  212.0 24.3 %all-to-all-done = bf16[4,64,4096]{2,1,0:T(8,128)(2,1)} async-done(((bf16[4,64,4096]{2,1,0:T(8,128)(2,1)}), bf16[4,64,4096]{2,1,0:T(8,128)(2,1)}, u32[]{:S(2)}, u32[]{:S(2)}) %all-to-all-start) | async-done | bytes 2097184 | tf_op jit(solution)/shard_map/all_to_all | solution.py:34
  236.4 2.1 convert_reduce_fusion
  238.9 2.1 convolution_convert_fusion.6
  241.0 4.4 reshape.227
  245.4 269.1 %all_to_all.15 = bf16[128,2,4096]{2,1,0:T(2,128)(2,1)S(1)} all-to-all(bf16[128,2,4096]{2,1,0:T(2,128)(2,1)} %reshape.227), channel_id=1, replica_groups=mesh['grp'=2,'sp'=32,'tp'=4] {'sp','tp'}, dimensions={0} | all-to-all | bytes 4194304 | tf_op jit(solution)/shard_map/all_to_all | solution.py:239
  515.8 2.5 fusion.44
  518.4 7.6 %convolution_convert_fusion.5 = bf16[128,2,4096]{2,0,1:T(8,128)(2,1)} fusion(bf16[1,192,4096]{2,1,0:T(8,128)(2,1)} %param.43, bf16[1,4096,192]{1,2,0:T(8,128)(2,1)} %param.42, bf16[128,2,4096]{2,1,0:T(2,128)(2,1)} %copy-done.1, f32[128,1,2,192]{0,3,2,1:T(8,128)S(1)} %fusion.44), kind=kOutput, calls=%fused_computation.55 | convolution fusion | flops 806649856 | bytes 7536640 | tf_op jit(solution)/shard_map/sxcf,xfd->sxcd/dot_general | solution.py:247
  526.0 5.1 copy.81
  531.1 10.9 %all-to-all-start.2 = ((bf16[128,2,4096]{2,1,0:T(2,128)(2,1)}), bf16[128,2,4096]{2,1,0:T(2,128)(2,1)}, u32[]{:S(2)}, u32[]{:S(2)}) async-start(bf16[128,2,4096]{2,1,0:T(2,128)(2,1)} %copy.81), calls=%async_computation.3 | async-start | bytes 4194304 | tf_op jit(solution)/shard_map/all_to_all | solution.py:250
  542.9 44.0 %all-gather.5.cloned.1.call-done = bf16[256,4096]{1,0:T(8,128)(2,1)} async-done(((bf16[64,4096]{1,0:T(8,128)(2,1)}), bf16[256,4096]{1,0:T(8,128)(2,1)}) %all-gather.5.cloned.1.call-update) | async-done | bytes 2097168 | tf_op jit(solution)/shard_map/all_gather | solution.py:210
  586.9 2.5 fusion.105
  589.5 4.8 convolution_convert_fusion.4
  595.1 43.8 %all-to-all-done.2 = bf16[128,2,4096]{2,1,0:T(2,128)(2,1)} async-done(((bf16[128,2,4096]{2,1,0:T(2,128)(2,1)}), bf16[128,2,4096]{2,1,0:T(2,128)(2,1)}, u32[]{:S(2)}, u32[]{:S(2)}) %all-to-all-start.2) | async-done | bytes 2097184 | tf_op jit(solution)/shard_map/all_to_all | solution.py:250
  638.9 4.1 reshape.232
  643.0 5.1 gather_fusion
  648.1 3.4 reshape.233
  651.4 5.7 multiply_reduce_fusion
  657.1 2.3 fusion.79
  (143 shorter events, 47.6 us)
Async XLA Ops:
  6.5 197.7 %copy-start = (bf16[256,4096]{1,0:T(8,128)(2,1)S(1)}, bf16[256,4096]{1,0:T(8,128)(2,1)}, u32[]{:S(2)}) copy-start(bf16[256,4096]{1,0:T(8,128)(2,1)} %param.34) | copy-start | bytes 6291460
  6.6 4.0 copy-start.10
  6.6 4.1 copy-start.9
  6.6 116.5 %all-gather.3.cloned.1.call-start = ((), (), s32[]{:S(2)}) async-start(), calls=%async_computation.4 | async-start | bytes 9732096 | tf_op jit(solution)/shard_map/all_gather | solution.py:20
  142.7 3.7 copy-start.2
  142.7 3.7 copy-start.3
  142.7 3.7 copy-start.5
  142.7 3.7 copy-start.6
  155.8 1.6 copy-start.7
  157.5 1.6 copy-start.11
  159.1 0.9 copy-start.12
  206.4 4.8 copy-start.14
  206.4 29.9 %all-to-all-start = ((bf16[4,64,4096]{2,1,0:T(8,128)(2,1)}), bf16[4,64,4096]{2,1,0:T(8,128)(2,1)}, u32[]{:S(2)}, u32[]{:S(2)}) async-start(bf16[4,64,4096]{2,1,0:T(8,128)(2,1)} %bitcast.123), calls=%async_computation | async-start | bytes 4194304 | tf_op jit(solution)/shard_map/all_to_all | solution.py:34
  211.3 27.2 %copy-start.8 = (bf16[64,4096]{1,0:T(8,128)(2,1)S(1)}, bf16[64,4096]{1,0:T(8,128)(2,1)}, u32[]{:S(2)}) copy-start(bf16[64,4096]{1,0:T(8,128)(2,1)} %param.36) | copy-start | bytes 1572868
  212.0 26.7 %copy-start.13 = (f32[4096]{0:T(1024)S(1)}, f32[4096]{0:T(1024)}, u32[]{:S(2)}) copy-start(f32[4096]{0:T(1024)} %param.37) | copy-start | bytes 49156
  238.9 6.5 copy-start.4
  245.4 270.4 %copy-start.16 = (bf16[1,4096,192]{1,2,0:T(8,128)(2,1)S(1)}, bf16[1,4096,192]{1,2,0:T(8,128)(2,1)}, u32[]{:S(2)}) copy-start(bf16[1,4096,192]{1,2,0:T(8,128)(2,1)} %param.41) | copy-start | bytes 4718596
  514.5 1.3 copy-start.1
  531.1 107.8 %all-to-all-start.2 = ((bf16[128,2,4096]{2,1,0:T(2,128)(2,1)}), bf16[128,2,4096]{2,1,0:T(2,128)(2,1)}, u32[]{:S(2)}, u32[]{:S(2)}) async-start(bf16[128,2,4096]{2,1,0:T(2,128)(2,1)} %copy.81), calls=%async_computation.3 | async-start | bytes 4194304 | tf_op jit(solution)/shard_map/all_to_all | solution.py:250
  542.0 44.9 %all-gather.5.cloned.1.call-start = ((), (), s32[]{:S(2)}) async-start(), calls=%async_computation.5 | async-start | bytes 2621440 | tf_op jit(solution)/shard_map/all_gather | solution.py:210
  542.8 114.3 %reduce-scatter.2.cloned.1.call-start = ((), (), s32[]{:S(2)}) async-start(), calls=%async_computation.6 | async-start | bytes 2621440 | tf_op jit(solution)/shard_map/reduce_scatter | solution.py:215
  594.3 0.7 copy-start.15
Sparse Core Ops, SparseCore 0:
  10.7 112.3 all-gather.2
  544.7 42.1 all-gather.4
  594.5 40.4 reduce-scatter.1
where the time goes:
time: 674 us; the launch traced here: 666 us
  blocking collectives  269 us (40%)
  waiting for transfers between devices  224 us (33%)
  local copies, waits for them, and re-layouts  58.7 us (9%)
  other arithmetic  39.3 us (6%)
  matrix products  33.3 us (5%)
  starting transfers between devices  15.8 us (2%)
  between operations  13.5 us (2%)
  loops' own time  11.8 us (2%)
    all_to_all x1, blocking collectives, body(): lax.all_to_all(outgoing, ('sp', 'tp'), split_axis=0, concat_axis=0, tiled...  269 us
    all_gather x1, waiting for transfers between devices, sent_together(): whole, at, outs = (lax.all_gather(both, axis, axis=dim, tiled=True), 0, [])  111 us
    all_gather x1, waiting for transfers between devices, body(): piece = lax.all_gather(normed, 'tp', axis=0, tiled=True)  44 us
    all_to_all x1, waiting for transfers between devices, body(): lax.all_to_all(finished.reshape(incoming.shape), ('sp', 'tp'), split_axis...  43.8 us
    all_to_all x1, waiting for transfers between devices, summed_on_arrival(): blocks = lax.all_to_all(split_up(array, dim, peers), axis, 0, 0, tiled=True)  24.3 us
    reduce_min x16, other arithmetic, one_block(): jnp.min(key_pos) <= last_pos  23.3 us
    unnamed x35, local copies, waits for them, and re-layouts  15.4 us
  transfers between devices with their start and end apart: 5, of which 4 were waited for; matrix products, arithmetic and copies ran while one was open for 4% of the time, Pallas kernels for 0%

commit v1 on v0

v1 whole, which is shorter than its diff:
```python
import functools
import math

import jax
import jax.numpy as jnp
import numpy as np
from jax import lax
from jax.experimental import pallas as pl
from jax.experimental.pallas import tpu as pltpu
from jax.sharding import PartitionSpec as P

ROPE = 64
WIDE_HEAD_SIZE = 128
NARROW_HEAD_SIZE = 64
LANES = 128


EPS = 1e-06
ROPE_BASE = 10000.0
NEG_FILL = -1e30
LOG2E = 1.4426950408889634


def split_up(array, dim, peers):
    before, after = (array.shape[:dim], array.shape[dim + 1 :])
    return jnp.moveaxis(array.reshape(*before, peers, -1, *after), dim, 0)


def summed_on_arrival(array, axis, dim):
    peers = lax.axis_size(axis)
    blocks = lax.all_to_all(split_up(array, dim, peers), axis, 0, 0, tiled=True)
    return jnp.sum(blocks.astype(jnp.float32), axis=0)


def rms_scale(values, gain):
    return values * lax.rsqrt(jnp.mean(values * values, axis=-1, keepdims=True) + EPS) * gain


def angle_tables(positions):
    half = ROPE // 2
    inverse = ROPE_BASE ** (-np.arange(half) * 2.0 / ROPE)
    angles = positions[:, None] * np.concatenate([inverse, inverse])[None, :]
    pad = ((0, 0), (0, LANES - ROPE))
    return (
        np.pad(np.cos(angles), pad).astype(np.float32),
        np.pad(np.sin(angles), pad).astype(np.float32),
    )


def attention_kernel(
    n_sp,
    n_tp,
    latent_ref,
    rope_key_ref,
    wide_query_ref,
    narrow_query_ref,
    wide_key_ref,
    wide_value_ref,
    narrow_key_ref,
    narrow_value_ref,
    gain_ref,
    local_cos_ref,
    local_sin_ref,
    base_cos_ref,
    base_sin_ref,
    out_ref,
    rows_buf,
    queries,
    narrow_weight,
    top,
    mixed,
    z_send,
    z_recv,
    x_send,
    x_recv,
    d_send,
    d_recv,
):
    tokens, width = latent_ref.shape
    quarter = tokens // n_tp
    zn = n_sp // 2
    steps_up = zn // 2
    steps_down = zn - 1 - steps_up
    me = lax.axis_index("sp")
    x = lax.axis_index("tp")
    z = me // 2
    core = lax.rem(me, 2)
    right = lax.rem(x + 1, n_tp)
    left = lax.rem(x + n_tp - 1, n_tp)
    up = lax.rem(z + 1, zn)
    down = lax.rem(z + zn - 1, zn)
    partner = z * 2 + 1 - core

    barrier = pltpu.get_barrier_semaphore()
    for place in ({"sp": up * 2 + core}, {"sp": down * 2 + core}, {"sp": partner}, {"tp": left}, {"tp": right}):
        pl.semaphore_signal(barrier, inc=1, device_id=place, device_id_type=pl.DeviceIdType.MESH)

    lane = lax.broadcasted_iota(jnp.int32, (tokens, LANES), 1)
    low = lane < ROPE
    lc, ls = local_cos_ref[...], local_sin_ref[...]
    bc, bs = base_cos_ref[pl.ds(me, 1), :], base_sin_ref[pl.ds(me, 1), :]
    cosine = lc * bc - ls * bs
    sine = jnp.where(lane < ROPE // 2, -1.0, 1.0) * (ls * bc + lc * bs)

    def turn(v):
        other = jnp.where(
            lane < ROPE // 2, pltpu.roll(v, LANES - ROPE // 2, 1), pltpu.roll(v, ROPE // 2, 1)
        )
        return (v * cosine + other * sine).astype(jnp.bfloat16)

    lat = latent_ref[...].astype(jnp.float32)
    normed = rms_scale(lat, gain_ref[...]).astype(jnp.bfloat16)
    rope = rope_key_ref[...].astype(jnp.float32)
    turned = turn(jnp.concatenate([rope, jnp.zeros_like(rope)], axis=1))
    for q in range(n_tp):
        rows_buf[me, q, :, :width] = normed[q * quarter : (q + 1) * quarter]
        rows_buf[me, q, :, width:] = turned[q * quarter : (q + 1) * quarter]

    t1 = wide_query_ref[:, LANES : 2 * LANES].astype(jnp.float32)
    t2 = wide_query_ref[:, 2 * LANES :].astype(jnp.float32)
    n0 = narrow_query_ref[:, :LANES].astype(jnp.float32)
    n1 = narrow_query_ref[:, LANES:].astype(jnp.float32)
    half = LANES // 2
    queries[0, :, :LANES] = wide_query_ref[:, :LANES]
    queries[0, :, LANES:] = turn(t1)
    queries[1, :, :LANES] = pltpu.roll(jnp.where(low, t2, t1), half, 1).astype(jnp.bfloat16)
    queries[1, :, LANES:] = turn(pltpu.roll(t2, half, 1))
    queries[2, :, :LANES] = jnp.where(low, n0, 0.0).astype(jnp.bfloat16)
    queries[2, :, LANES:] = turn(pltpu.roll(n0, half, 1))
    queries[3, :, :LANES] = pltpu.roll(jnp.where(low, n1, 0.0), half, 1).astype(jnp.bfloat16)
    queries[3, :, LANES:] = turn(pltpu.roll(n1, half, 1))
    narrow_weight[:, :LANES] = narrow_key_ref[...]
    narrow_weight[:, LANES:] = narrow_value_ref[...]
    top[...] = jnp.full(top.shape, NEG_FILL, jnp.float32)
    mixed[...] = jnp.zeros(mixed.shape, jnp.float32)
    pl.semaphore_wait(barrier, 5)

    def along_z(d, k, j):
        block = jnp.where(d == 0, z - k + zn, z + k) % zn
        target = jnp.where(d == 0, up, down)
        q = lax.rem(x + j, n_tp)
        spot = rows_buf.at[block * 2 + core, q]
        return pltpu.make_async_remote_copy(
            src_ref=spot,
            dst_ref=spot,
            send_sem=z_send.at[d, k, j],
            recv_sem=z_recv.at[d, k + 1, j],
            device_id={"sp": target * 2 + core},
            device_id_type=pl.DeviceIdType.MESH,
        )

    def along_x(d, k, j):
        block = jnp.where(d == 0, z - k + zn, z + k) % zn
        q = lax.rem(x + j, n_tp)
        spot = rows_buf.at[block * 2 + core, q]
        return pltpu.make_async_remote_copy(
            src_ref=spot,
            dst_ref=spot,
            send_sem=x_send.at[d, k, j],
            recv_sem=x_recv.at[d, k, j],
            device_id={"tp": right if j == 0 else left},
            device_id_type=pl.DeviceIdType.MESH,
        )

    def to_partner(d, k):
        block = jnp.where(d == 0, z - k + zn, z + k) % zn
        spot = rows_buf.at[block * 2 + core]
        return pltpu.make_async_remote_copy(
            src_ref=spot,
            dst_ref=spot,
            send_sem=d_send.at[d, k],
            recv_sem=d_recv.at[d, k],
            device_id={"sp": partner},
            device_id_type=pl.DeviceIdType.MESH,
        )

    def arrives(d, k):
        going_up = (k <= z) & (k <= steps_up)
        going_down = ((z + k) % zn < steps_down) & (k <= steps_down)
        return jnp.where(d == 0, going_up, going_down)

    def goes_on(d, k):
        going_up = (k <= z) & (k < steps_up) & (z + 1 < zn)
        going_down = ((z + k) % zn < steps_down) & (k < steps_down)
        return jnp.where(d == 0, going_up, going_down)

    def seen(d, k):
        going_up = (k <= z) & (k <= steps_up)
        going_down = (z + k >= zn) & (z + k - zn < steps_down) & (k <= steps_down)
        return (k >= 1) & jnp.where(d == 0, going_up, going_down)

    wide_factor = (WIDE_HEAD_SIZE + ROPE) ** (-0.5) * LOG2E
    narrow_factor = (NARROW_HEAD_SIZE + ROPE) ** (-0.5) * LOG2E

    def attend(plane, own):
        rows = rows_buf[pl.ds(plane * 2, 2)].reshape(2 * tokens, width + LANES)
        latents, turned_rows = rows[:, :width], rows[:, width:]
        keys = 2 * tokens
        ones = jnp.ones((keys, LANES), jnp.bfloat16)

        def up_from(weight):
            return jnp.dot(latents, weight[...], preferred_element_type=jnp.float32).astype(jnp.bfloat16)

        wide_k, wide_v, narrow = up_from(wide_key_ref), up_from(wide_value_ref), up_from(narrow_weight)
        narrow_k = jnp.concatenate([narrow[:, :LANES], turned_rows], axis=1)
        narrow_v = jnp.concatenate([narrow[:, LANES:], ones], axis=1)
        if own:
            gap = lax.broadcasted_iota(jnp.int32, (tokens, keys), 1) - lax.broadcasted_iota(
                jnp.int32, (tokens, keys), 0
            )
            visible = gap <= core * tokens
        for h in range(4):
            if h < 2:
                at = slice(h * LANES, (h + 1) * LANES)
                k_h = jnp.concatenate([wide_k[:, at], turned_rows], axis=1)
                v_h = jnp.concatenate([wide_v[:, at], ones], axis=1)
            else:
                k_h, v_h = narrow_k, narrow_v
            scores = lax.dot_general(
                queries[h], k_h, (((1,), (1,)), ((), ())), preferred_element_type=jnp.float32
            ) * (wide_factor if h < 2 else narrow_factor)
            if own:
                scores = jnp.where(visible, scores, NEG_FILL)
            old = top[h]
            new = jnp.maximum(old, jnp.max(scores, axis=1, keepdims=True))
            top[h] = new
            weights = jnp.exp2(scores - jnp.concatenate([new] * (keys // LANES), axis=1)).astype(jnp.bfloat16)
            fading = jnp.exp2(old - new)
            mixed[h] = mixed[h] * jnp.concatenate([fading, fading], axis=1) + jnp.dot(
                weights, v_h, preferred_element_type=jnp.float32
            )

    to_partner(0, 0).start()
    for d in range(2):

        @pl.when(goes_on(d, 0))
        def _():
            for j in range(2):
                along_z(d, 0, j).start()

    to_partner(0, 0).wait_recv()

    attend(z, True)

    def one_step(k, carry):
        def forward(d, c):
            @pl.when(arrives(d, k))
            def _():
                for j in range(2):
                    along_z(d, k - 1, j).wait_recv()

            @pl.when(goes_on(d, k))
            def _():
                for j in range(2):
                    along_z(d, k, j).start()

            @pl.when(seen(d, k))
            def _():
                for j in range(2):
                    along_x(d, k, j).start()

            @pl.when(seen(d, k - 1))
            def _():
                for j in range(2):
                    along_x(d, k - 1, j).wait_recv()
                to_partner(d, k - 1).start()

            return c

        lax.fori_loop(0, 2, forward, 0)

        def work(d, c):
            @pl.when(seen(d, k - 2))
            def _():
                to_partner(d, k - 2).wait_recv()
                attend(jnp.where(d == 0, z - k + 2, z + k - 2 - zn), False)

            return c

        lax.fori_loop(0, 2, work, 0)
        return carry

    lax.fori_loop(1, steps_up + 3, one_step, 0)

    to_partner(0, 0).wait_send()

    def settle(k, carry):
        def both(d, c):
            @pl.when(goes_on(d, k))
            def _():
                for j in range(2):
                    along_z(d, k, j).wait_send()

            @pl.when(seen(d, k))
            def _():
                for j in range(2):
                    along_x(d, k, j).wait_send()
                to_partner(d, k).wait_send()

            return c

        return lax.fori_loop(0, 2, both, carry)

    lax.fori_loop(0, steps_up + 1, settle, 0)

    for h in range(2):
        out_ref[:, h * LANES : (h + 1) * LANES] = (mixed[h, :, :LANES] / mixed[h, :, LANES:]).astype(
            out_ref.dtype
        )
    out_ref[:, 2 * LANES :] = jnp.where(
        low, mixed[2, :, :LANES] / mixed[2, :, LANES:], mixed[3, :, :LANES] / mixed[3, :, LANES:]
    ).astype(out_ref.dtype)


def attention(
    latent, rope_key, wide_query, narrow_query, wide_key, wide_value, narrow_key, narrow_value, gain
):
    tokens, width = latent.shape
    n_sp, n_tp = lax.axis_size("sp"), lax.axis_size("tp")
    zn = n_sp // 2
    assert n_sp % 4 == 0 and n_tp == 4 and wide_query.shape[1] == 3 * LANES
    assert narrow_query.shape[1] == 2 * LANES and zn >= 4
    local_cos, local_sin = angle_tables(np.arange(tokens, dtype=np.float64))
    base_cos, base_sin = angle_tables(np.arange(n_sp, dtype=np.float64) * tokens)
    hops = zn // 2 + 1
    dma = pltpu.SemaphoreType.DMA
    vmem = pl.BlockSpec(memory_space=pltpu.VMEM)
    return pl.pallas_call(
        functools.partial(attention_kernel, n_sp, n_tp),
        out_shape=jax.ShapeDtypeStruct((tokens, 3 * LANES), jnp.bfloat16),
        in_specs=[vmem] * 13,
        out_specs=vmem,
        scratch_shapes=[
            pltpu.VMEM((n_sp, n_tp, tokens // n_tp, width + LANES), jnp.bfloat16),
            pltpu.VMEM((4, tokens, 2 * LANES), jnp.bfloat16),
            pltpu.VMEM((width, 2 * LANES), jnp.bfloat16),
            pltpu.VMEM((4, tokens, LANES), jnp.float32),
            pltpu.VMEM((4, tokens, 2 * LANES), jnp.float32),
            dma((2, hops, 2)),
            dma((2, hops + 1, 2)),
            dma((2, hops, 2)),
            dma((2, hops, 2)),
            dma((2, hops)),
            dma((2, hops)),
        ],
        compiler_params=pltpu.CompilerParams(
            collective_id=0, has_side_effects=True, vmem_limit_bytes=48 * 1024 * 1024
        ),
    )(
        latent,
        rope_key,
        wide_query,
        narrow_query,
        wide_key,
        wide_value,
        narrow_key,
        narrow_value,
        gain.reshape(1, width),
        local_cos,
        local_sin,
        base_cos,
        base_sin,
    )


def body(
    latent,
    rope_key,
    wide_query,
    narrow_query,
    wide_key_weight,
    wide_value_weight,
    narrow_key_weight,
    narrow_value_weight,
    latent_norm_scale,
    out_wide,
    out_narrow,
    residual,
    ffn_gain,
    shared_gate,
    shared_up,
    shared_down,
    expert_gate,
    expert_up,
    expert_down,
    routes,
    route_weights,
):
    mix = attention(
        latent,
        rope_key,
        wide_query,
        narrow_query,
        wide_key_weight,
        wide_value_weight,
        narrow_key_weight,
        narrow_value_weight,
        latent_norm_scale,
    )
    wide_cols = out_wide.shape[0]
    wide_mix, narrow_mix = mix[:, :wide_cols], mix[:, wide_cols:]
    projected = summed_on_arrival(
        (
            jnp.dot(wide_mix, out_wide, preferred_element_type=jnp.float32)
            + jnp.dot(narrow_mix, out_narrow, preferred_element_type=jnp.float32)
        ).astype(jnp.bfloat16),
        "tp",
        0,
    )
    stream = (residual.astype(jnp.float32) + projected).astype(jnp.bfloat16)
    normed = rms_scale(stream.astype(jnp.float32), ffn_gain).astype(jnp.bfloat16)
    piece = lax.all_gather(normed, "tp", axis=0, tiled=True)
    gate_part = jnp.dot(piece, shared_gate, preferred_element_type=jnp.float32)
    up_part = jnp.dot(piece, shared_up, preferred_element_type=jnp.float32)
    active = (jax.nn.silu(gate_part) * up_part).astype(jnp.bfloat16)
    shared_terms = jnp.dot(active, shared_down, preferred_element_type=jnp.float32)
    shared = lax.psum_scatter(
        shared_terms.astype(jnp.bfloat16), "tp", scatter_dimension=0, tiled=True
    ).astype(jnp.float32)
    rows_here, top_count = routes.shape
    local_experts = expert_gate.shape[0]
    experts_all = local_experts * lax.axis_size(("sp", "tp"))
    capacity = max(2, 2 * top_count * rows_here // experts_all)
    model_width = normed.shape[1]
    flat_routes = routes.reshape(-1)
    assigned = flat_routes.shape[0]
    choose = (flat_routes[:, None] == jnp.arange(experts_all, dtype=jnp.int32)[None, :]).astype(
        jnp.float32
    )
    lower_mask = (jnp.arange(assigned)[:, None] > jnp.arange(assigned)[None, :]).astype(jnp.float32)
    earlier = jnp.dot(lower_mask, choose, precision=lax.Precision.HIGHEST)
    slots = jnp.sum(earlier * choose, axis=1).astype(jnp.int32)
    target = flat_routes * capacity + slots
    send_map = jnp.any(
        target.reshape(rows_here, top_count)[None, :, :]
        == jnp.arange(experts_all * capacity, dtype=jnp.int32)[:, None, None],
        axis=2,
    ).astype(jnp.bfloat16)
    outgoing = jnp.dot(send_map, normed, preferred_element_type=jnp.float32).astype(jnp.bfloat16)
    incoming = lax.all_to_all(outgoing, ("sp", "tp"), split_axis=0, concat_axis=0, tiled=True)
    finished = []
    for x in range(local_experts):
        rows = incoming
        if local_experts > 1:
            rows = incoming.reshape(-1, local_experts, capacity, model_width)[:, x].reshape(-1, model_width)
        gate_part = jnp.dot(rows, expert_gate[x], preferred_element_type=jnp.float32)
        up_part = jnp.dot(rows, expert_up[x], preferred_element_type=jnp.float32)
        active = (jax.nn.silu(gate_part) * up_part).astype(jnp.bfloat16)
        finished.append(
            jnp.dot(active, expert_down[x], preferred_element_type=jnp.float32).astype(jnp.bfloat16)
        )
    if local_experts > 1:
        stacked = jnp.stack([f.reshape(-1, capacity, model_width) for f in finished], axis=1)
        finished = [stacked.reshape(-1, model_width)]
    returned = lax.all_to_all(finished[0], ("sp", "tp"), split_axis=0, concat_axis=0, tiled=True)
    chosen = target.reshape(rows_here, top_count)
    places = jnp.arange(experts_all * capacity, dtype=jnp.int32)[None, :]
    routed = jnp.zeros((rows_here, model_width), jnp.float32)
    for c in range(top_count):
        pick = (chosen[:, c : c + 1] == places).astype(jnp.bfloat16)
        routed = routed + route_weights[:, c : c + 1] * jnp.dot(
            pick, returned, preferred_element_type=jnp.float32
        )
    return (stream.astype(jnp.float32) + shared + routed).astype(jnp.bfloat16)


def solution(mesh):
    placed = (
        P(("grp", "sp"), None),
        P(("grp", "sp"), None),
        P(("grp", "sp"), "tp"),
        P(("grp", "sp"), "tp"),
        P(None, "tp"),
        P(None, "tp"),
        P(None, "tp"),
        P(None, "tp"),
        P(),
        P("tp", None),
        P("tp", None),
        P(("grp", "sp", "tp"), None),
        P(),
        P(None, "tp"),
        P(None, "tp"),
        P("tp", None),
        P(("sp", "tp"), None, None),
        P(("sp", "tp"), None, None),
        P(("sp", "tp"), None, None),
        P(("grp", "sp", "tp"), None),
        P(("grp", "sp", "tp"), None),
    )
    return jax.shard_map(
        body, mesh=mesh, in_specs=placed, out_specs=P(("grp", "sp", "tp"), None), check_vma=False
    )
```

time: 674 us -> 389 us (0.58)
  blocking collectives: 269 us -> 134 us
  waiting for transfers between devices: 224 us -> 110 us
  Pallas kernels: 0 us -> 52 us
  other arithmetic: 39.3 us -> 2.64 us
  local copies, waits for them, and re-layouts: 58.7 us -> 29.6 us
  loops' own time: 11.8 us -> 0 us
    all_to_all x1, blocking collectives: 269 us -> 134 us  [body(): lax.all_to_all(outgoing, ('sp', 'tp'), split_axis=0, concat_axis=0, tiled...]
    all_gather x1 -> x0, waiting for transfers between devices: 111 us -> none  [sent_together(): whole, at, outs = (lax.all_gather(both, axis, axis=dim, tiled=True), 0, [])]
    pallas_call x0 -> x1, Pallas kernels: none -> 52 us  [attention(): pl.pallas_call(functools.partial(attention_kernel, n_sp, n_tp), out_shape...]
    reduce_min x16 -> x0, other arithmetic: 23.3 us -> none  [one_block(): jnp.min(key_pos) <= last_pos]
    all_to_all x0 -> x4, local copies, waits for them, and re-layouts: none -> 17.1 us  [the longest x2 8.55 us: body(): lax.all_to_all(finished[0], ('sp', 'tp'), split_axis=0, concat_axis=0, ti...]
    another operation x17 -> x0, loops' own time: 11.8 us -> none  [the longest x1 11.4 us: body(): final = lax.fori_loop(0, length_rows // block, one_block, initial)]
    slice x3 -> x0, local copies, waits for them, and re-layouts: 10.1 us -> none  [the longest x2 10.1 us: sent_together(): outs.append(lax.slice_in_dim(whole, at, at + a.shape[along], axis=along))]
    iota x17 -> x0, local copies, waits for them, and re-layouts: 9.91 us -> none  [the longest x16 9.3 us: body(): own_pos = seq_index * tok_dev + jnp.arange(tok_dev, dtype=jnp.int32)]
  transfers between devices with their start and end apart: 5 -> 4, of which waited for: 4 -> 3; matrix products, arithmetic and copies ran while one was open for 4% -> 3% of each run, Pallas kernels for 0% -> 0%
where the time goes in v1:
time: 389 us; the launch traced here: 386 us
  blocking collectives  134 us (34%)
  waiting for transfers between devices  110 us (28%)
  Pallas kernels  52 us (13%)
  local copies, waits for them, and re-layouts  29.6 us (8%)
  matrix products  28.3 us (7%)
  starting transfers between devices  15.7 us (4%)
  between operations  13.6 us (3%)
    all_to_all x1, blocking collectives, body(): lax.all_to_all(outgoing, ('sp', 'tp'), split_axis=0, concat_axis=0, tiled...  134 us
    pallas_call x1, Pallas kernels, attention(): pl.pallas_call(functools.partial(attention_kernel, n_sp, n_tp), out_shape...  52 us
    all_gather x1, waiting for transfers between devices, body(): piece = lax.all_gather(normed, 'tp', axis=0, tiled=True)  44.9 us
    all_to_all x1, waiting for transfers between devices, body(): lax.all_to_all(finished[0], ('sp', 'tp'), split_axis=0, concat_axis=0, ti...  43 us
    all_to_all x1, waiting for transfers between devices, summed_on_arrival(): blocks = lax.all_to_all(split_up(array, dim, peers), axis, 0, 0, tiled=True)  21.6 us
    unnamed x40, local copies, waits for them, and re-layouts  12.2 us
    all_to_all x1, starting transfers between devices, body(): lax.all_to_all(finished[0], ('sp', 'tp'), split_axis=0, concat_axis=0, ti...  10.9 us
    all_to_all x2, local copies, waits for them, and re-layouts, body(): lax.all_to_all(finished[0], ('sp', 'tp'), split_axis=0, concat_axis=0, ti...  8.55 us
  transfers between devices with their start and end apart: 4, of which 3 were waited for; matrix products, arithmetic and copies ran while one was open for 3% of the time, Pallas kernels for 0%

profile of v1, /device:TPU:35, one launch (start us, length us, event | category | flops | bytes accessed | tf_op | source)
XLA Modules:
  0.0 386.4 jit_solution(1060183994529524657)
XLA Ops:
  6.6 1.0 copy.39.rope_key_ref
  7.6 0.9 copy-done.1
  8.5 0.9 copy-done.2
  9.5 0.9 copy-done.3
  10.4 0.9 copy-done.4
  11.4 0.9 copy-done.5
  12.3 0.9 copy-done.6
  13.2 0.9 copy-done.7
  14.1 0.9 copy-done.8
  15.0 0.9 copy-done.9
  15.9 0.7 copy-done.10
  18.0 52.0 %shard_map.235 = bf16[256,384]{1,0:T(8,128)(2,1)S(1)} custom-call(bf16[256,512]{1,0:T(8,128)(2,1)S(1)} %copy-done.1, bf16[256,64]{1,0:T(8,128)(2,1)S(1)} %copy.39.rope_key_ref, bf16[256,384]{1,0:T(8,128)(2,1)S(1)} %copy-done.4, bf16[256,256]{1,0:T(8,128)(2,1)S(1)} %copy-done.5, bf16[512,256]{1,0:T(8,128)(2,1)S(1)} %copy-done.2, ...), custom_call_target="tpu_custom_call" | custom-call | tf_op jit(solution)/shard_map/pallas_call | solution.py:328
  70.7 2.1 fusion
  72.8 4.7 %all-to-all-start = ((bf16[4,64,4096]{2,1,0:T(8,128)(2,1)}), bf16[4,64,4096]{2,1,0:T(8,128)(2,1)}, u32[]{:S(2)}, u32[]{:S(2)}) async-start(bf16[4,64,4096]{2,1,0:T(8,128)(2,1)} %bitcast.39), calls=%async_computation | async-start | bytes 4194304 | tf_op jit(solution)/shard_map/all_to_all | solution.py:31
  78.3 21.6 %all-to-all-done = bf16[4,64,4096]{2,1,0:T(8,128)(2,1)} async-done(((bf16[4,64,4096]{2,1,0:T(8,128)(2,1)}), bf16[4,64,4096]{2,1,0:T(8,128)(2,1)}, u32[]{:S(2)}, u32[]{:S(2)}) %all-to-all-start) | async-done | bytes 2097184 | tf_op jit(solution)/shard_map/all_to_all | solution.py:31
  99.9 2.1 convert_reduce_fusion
  102.4 2.1 convolution_convert_fusion.2
  104.5 4.4 %all_to_all.20 = bf16[128,2,4096]{2,1,0:T(2,128)(2,1)} reshape(bf16[256,4096]{1,0:T(8,128)(2,1)} %convolution_convert_fusion.2) | data formatting | bytes 4194304 | tf_op jit(solution)/shard_map/all_to_all | solution.py:440
  108.9 134.4 %all_to_all.29 = bf16[128,2,4096]{2,1,0:T(2,128)(2,1)} all-to-all(bf16[128,2,4096]{2,1,0:T(2,128)(2,1)} %all_to_all.20), channel_id=1, replica_groups=mesh['grp'=2,'sp'=32,'tp'=4] {'sp','tp'}, dimensions={0} | all-to-all | bytes 4194304 | tf_op jit(solution)/shard_map/all_to_all | solution.py:440
  243.3 4.1 %all_to_all.22 = bf16[256,4096]{1,0:T(8,128)(2,1)} reshape(bf16[128,2,4096]{2,1,0:T(2,128)(2,1)} %all_to_all.29) | data formatting | bytes 4194304 | tf_op jit(solution)/shard_map/all_to_all | solution.py:440
  247.4 2.9 fusion.7
  250.3 6.4 %convolution_convert_fusion.1 = bf16[256,4096]{1,0:T(8,128)(2,1)} fusion(bf16[1,192,4096]{2,1,0:T(8,128)(2,1)} %param.43, bf16[256,4096]{1,0:T(8,128)(2,1)} %all_to_all.22, bf16[1,4096,192]{1,2,0:T(8,128)(2,1)} %param.42, f32[256,192]{0,1:T(8,128)S(1)} %fusion.7), kind=kOutput, calls=%fused_computation.3 | convolution fusion | flops 806649856 | bytes 7536640 | tf_op jit(solution)/shard_map/dot_general | solution.py:450
  256.7 4.4 %all_to_all.23 = bf16[128,2,4096]{2,1,0:T(2,128)(2,1)} reshape(bf16[256,4096]{1,0:T(8,128)(2,1)} %convolution_convert_fusion.1) | data formatting | bytes 4194304 | tf_op jit(solution)/shard_map/all_to_all | solution.py:455
  261.1 10.9 %all-to-all-start.2 = ((bf16[128,2,4096]{2,1,0:T(2,128)(2,1)}), bf16[128,2,4096]{2,1,0:T(2,128)(2,1)}, u32[]{:S(2)}, u32[]{:S(2)}) async-start(bf16[128,2,4096]{2,1,0:T(2,128)(2,1)} %all_to_all.23), calls=%async_computation.3 | async-start | bytes 4194304 | tf_op jit(solution)/shard_map/all_to_all | solution.py:455
  272.1 0.7 all-gather.2.cloned.1.call-update
  272.9 44.9 %all-gather.2.cloned.1.call-done = bf16[256,4096]{1,0:T(8,128)(2,1)} async-done(((bf16[64,4096]{1,0:T(8,128)(2,1)}), bf16[256,4096]{1,0:T(8,128)(2,1)}) %all-gather.2.cloned.1.call-update) | async-done | bytes 2097168 | tf_op jit(solution)/shard_map/all_gather | solution.py:412
  317.8 2.5 fusion.43
  320.4 4.8 %convolution_convert_fusion = bf16[256,4096]{1,0:T(8,128)(2,1)} fusion(bf16[128,4096]{1,0:T(8,128)(2,1)} %param.40, bf16[256,4096]{1,0:T(8,128)(2,1)} %all-gather.2.cloned.1.call-done, bf16[4096,128]{1,0:T(8,128)(2,1)} %param.39, f32[256,128]{1,0:T(8,128)S(1)} %fusion.43), kind=kOutput, calls=%fused_computation.1 | convolution fusion | flops 538116096 | bytes 6422528 | tf_op jit(solution)/shard_map/dot_general | solution.py:416
  325.9 43.0 %all-to-all-done.2 = bf16[128,2,4096]{2,1,0:T(2,128)(2,1)} async-done(((bf16[128,2,4096]{2,1,0:T(2,128)(2,1)}), bf16[128,2,4096]{2,1,0:T(2,128)(2,1)}, u32[]{:S(2)}, u32[]{:S(2)}) %all-to-all-start.2) | async-done | bytes 2097184 | tf_op jit(solution)/shard_map/all_to_all | solution.py:455
  368.9 4.1 %all_to_all.25 = bf16[256,4096]{1,0:T(8,128)(2,1)} reshape(bf16[128,2,4096]{2,1,0:T(2,128)(2,1)} %all-to-all-done.2) | data formatting | bytes 4194304 | tf_op jit(solution)/shard_map/all_to_all | solution.py:455
  373.1 3.1 convolution_multiply_fusion.1
  376.2 3.4 fusion.3
  (46 shorter events, 4.1 us)
Async XLA Ops:
  6.5 64.1 %copy-start = (bf16[256,4096]{1,0:T(8,128)(2,1)S(1)}, bf16[256,4096]{1,0:T(8,128)(2,1)}, u32[]{:S(2)}) copy-start(bf16[256,4096]{1,0:T(8,128)(2,1)} %param.34) | copy-start | bytes 6291460
  7.6 1.0 copy-start.1
  8.5 0.9 copy-start.2
  9.5 0.9 copy-start.3
  10.4 0.9 copy-start.4
  11.4 0.9 copy-start.5
  12.3 0.9 copy-start.6
  13.2 0.9 copy-start.7
  14.1 0.9 copy-start.8
  15.0 0.9 copy-start.9
  15.9 0.7 copy-start.10
  16.6 0.7 copy-start.11
  17.3 0.7 copy-start.12
  18.0 52.0 %copy-start.14 = (bf16[128,4096]{1,0:T(8,128)(2,1)S(1)}, bf16[128,4096]{1,0:T(8,128)(2,1)}, u32[]{:S(2)}) copy-start(bf16[128,4096]{1,0:T(8,128)(2,1)} %param.35) | copy-start | bytes 3145732
  72.8 4.7 %copy-start.17 = (s32[64,2]{0,1:T(2,128)S(1)}, s32[64,2]{0,1:T(2,128)}, u32[]{:S(2)}) copy-start(s32[64,2]{0,1:T(2,128)} %param.44) | copy-start | bytes 1540
  72.8 27.0 %all-to-all-start = ((bf16[4,64,4096]{2,1,0:T(8,128)(2,1)}), bf16[4,64,4096]{2,1,0:T(8,128)(2,1)}, u32[]{:S(2)}, u32[]{:S(2)}) async-start(bf16[4,64,4096]{2,1,0:T(8,128)(2,1)} %bitcast.39), calls=%async_computation | async-start | bytes 4194304 | tf_op jit(solution)/shard_map/all_to_all | solution.py:31
  77.5 24.4 %copy-start.15 = (bf16[64,4096]{1,0:T(8,128)(2,1)S(1)}, bf16[64,4096]{1,0:T(8,128)(2,1)}, u32[]{:S(2)}) copy-start(bf16[64,4096]{1,0:T(8,128)(2,1)} %param.36) | copy-start | bytes 1572868
  78.3 23.9 %copy-start.16 = (f32[4096]{0:T(1024)S(1)}, f32[4096]{0:T(1024)}, u32[]{:S(2)}) copy-start(f32[4096]{0:T(1024)} %param.37) | copy-start | bytes 49156
  102.4 6.5 %copy-start.13 = (bf16[64,4096]{1,0:T(8,128)(2,1)}, bf16[64,4096]{1,0:T(8,128)(2,1)S(1)}, u32[]{:S(2)}) copy-start(bf16[64,4096]{1,0:T(8,128)(2,1)S(1)} %fusion.21) | copy-start | bytes 1572868
  261.1 107.8 %all-to-all-start.2 = ((bf16[128,2,4096]{2,1,0:T(2,128)(2,1)}), bf16[128,2,4096]{2,1,0:T(2,128)(2,1)}, u32[]{:S(2)}, u32[]{:S(2)}) async-start(bf16[128,2,4096]{2,1,0:T(2,128)(2,1)} %all_to_all.23), calls=%async_computation.3 | async-start | bytes 4194304 | tf_op jit(solution)/shard_map/all_to_all | solution.py:455
  272.0 45.8 %all-gather.2.cloned.1.call-start = ((), (), s32[]{:S(2)}) async-start(), calls=%async_computation.4 | async-start | bytes 2621440 | tf_op jit(solution)/shard_map/all_gather | solution.py:412
  272.8 103.4 %reduce-scatter.2.cloned.1.call-start = ((), (), s32[]{:S(2)}) async-start(), calls=%async_computation.5 | async-start | bytes 2621440 | tf_op jit(solution)/shard_map/reduce_scatter | solution.py:417
  325.2 0.7 copy-start.18
Sparse Core Ops, SparseCore 0:
  274.7 43.0 all-gather.1
  325.4 40.1 reduce-scatter.1

commit v2 on v1

--- a/solution.py
+++ b/solution.py
@@ -1,5 +1,4 @@
 import functools
-import math
 
 import jax
 import jax.numpy as jnp
@@ -19,17 +18,6 @@
 ROPE_BASE = 10000.0
 NEG_FILL = -1e30
 LOG2E = 1.4426950408889634
-
-
-def split_up(array, dim, peers):
-    before, after = (array.shape[:dim], array.shape[dim + 1 :])
-    return jnp.moveaxis(array.reshape(*before, peers, -1, *after), dim, 0)
-
-
-def summed_on_arrival(array, axis, dim):
-    peers = lax.axis_size(axis)
-    blocks = lax.all_to_all(split_up(array, dim, peers), axis, 0, 0, tiled=True)
-    return jnp.sum(blocks.astype(jnp.float32), axis=0)
 
 
 def rms_scale(values, gain):
@@ -50,25 +38,37 @@
 def attention_kernel(
     n_sp,
     n_tp,
+    latent_hbm,
+    rope_key_hbm,
+    wide_query_hbm,
+    narrow_query_hbm,
+    wide_key_hbm,
+    wide_value_hbm,
+    narrow_key_hbm,
+    narrow_value_hbm,
+    gain_hbm,
+    local_cos_hbm,
+    local_sin_hbm,
+    base_cos_hbm,
+    base_sin_hbm,
+    out_ref,
     latent_ref,
     rope_key_ref,
     wide_query_ref,
     narrow_query_ref,
     wide_key_ref,
     wide_value_ref,
-    narrow_key_ref,
-    narrow_value_ref,
     gain_ref,
     local_cos_ref,
     local_sin_ref,
     base_cos_ref,
     base_sin_ref,
-    out_ref,
     rows_buf,
     queries,
     narrow_weight,
     top,
     mixed,
+    fetch,
     z_send,
     z_recv,
     x_send,
@@ -76,7 +76,7 @@
     d_send,
     d_recv,
 ):
-    tokens, width = latent_ref.shape
+    tokens, width = latent_hbm.shape
     quarter = tokens // n_tp
     zn = n_sp // 2
     steps_up = zn // 2
@@ -91,10 +91,35 @@
     down = lax.rem(z + zn - 1, zn)
     partner = z * 2 + 1 - core
 
+    fetches = [
+        pltpu.make_async_copy(source, target, fetch.at[i])
+        for i, (source, target) in enumerate(
+            (
+                (latent_hbm, latent_ref),
+                (rope_key_hbm, rope_key_ref),
+                (gain_hbm, gain_ref),
+                (local_cos_hbm, local_cos_ref),
+                (local_sin_hbm, local_sin_ref),
+                (base_cos_hbm, base_cos_ref),
+                (base_sin_hbm, base_sin_ref),
+                (wide_query_hbm, wide_query_ref),
+                (narrow_query_hbm, narrow_query_ref),
+                (wide_key_hbm, wide_key_ref),
+                (wide_value_hbm, wide_value_ref),
+                (narrow_key_hbm, narrow_weight.at[:, pl.ds(0, LANES)]),
+                (narrow_value_hbm, narrow_weight.at[:, pl.ds(LANES, LANES)]),
+            )
+        )
+    ]
+    for copy in fetches:
+        copy.start()
+
     barrier = pltpu.get_barrier_semaphore()
     for place in ({"sp": up * 2 + core}, {"sp": down * 2 + core}, {"sp": partner}, {"tp": left}, {"tp": right}):
         pl.semaphore_signal(barrier, inc=1, device_id=place, device_id_type=pl.DeviceIdType.MESH)
 
+    for copy in fetches:
+        copy.wait()
     lane = lax.broadcasted_iota(jnp.int32, (tokens, LANES), 1)
     low = lane < ROPE
     lc, ls = local_cos_ref[...], local_sin_ref[...]
@@ -129,8 +154,6 @@
     queries[2, :, LANES:] = turn(pltpu.roll(n0, half, 1))
     queries[3, :, :LANES] = pltpu.roll(jnp.where(low, n1, 0.0), half, 1).astype(jnp.bfloat16)
     queries[3, :, LANES:] = turn(pltpu.roll(n1, half, 1))
-    narrow_weight[:, :LANES] = narrow_key_ref[...]
-    narrow_weight[:, LANES:] = narrow_value_ref[...]
     top[...] = jnp.full(top.shape, NEG_FILL, jnp.float32)
     mixed[...] = jnp.zeros(mixed.shape, jnp.float32)
     pl.semaphore_wait(barrier, 5)
@@ -328,14 +351,26 @@
     return pl.pallas_call(
         functools.partial(attention_kernel, n_sp, n_tp),
         out_shape=jax.ShapeDtypeStruct((tokens, 3 * LANES), jnp.bfloat16),
-        in_specs=[vmem] * 13,
+        in_specs=[pl.BlockSpec(memory_space=pltpu.HBM)] * 13,
         out_specs=vmem,
         scratch_shapes=[
+            pltpu.VMEM(latent.shape, jnp.bfloat16),
+            pltpu.VMEM(rope_key.shape, jnp.bfloat16),
+            pltpu.VMEM(wide_query.shape, jnp.bfloat16),
+            pltpu.VMEM(narrow_query.shape, jnp.bfloat16),
+            pltpu.VMEM(wide_key.shape, jnp.bfloat16),
+            pltpu.VMEM(wide_value.shape, jnp.bfloat16),
+            pltpu.VMEM((1, width), jnp.float32),
+            pltpu.VMEM(local_cos.shape, jnp.float32),
+            pltpu.VMEM(local_sin.shape, jnp.float32),
+            pltpu.VMEM(base_cos.shape, jnp.float32),
+            pltpu.VMEM(base_sin.shape, jnp.float32),
             pltpu.VMEM((n_sp, n_tp, tokens // n_tp, width + LANES), jnp.bfloat16),
             pltpu.VMEM((4, tokens, 2 * LANES), jnp.bfloat16),
             pltpu.VMEM((width, 2 * LANES), jnp.bfloat16),
             pltpu.VMEM((4, tokens, LANES), jnp.float32),
             pltpu.VMEM((4, tokens, 2 * LANES), jnp.float32),
+            dma((13,)),
             dma((2, hops, 2)),
             dma((2, hops + 1, 2)),
             dma((2, hops, 2)),
@@ -360,6 +395,427 @@
         local_sin,
         base_cos,
         base_sin,
+    )
+
+
+DELTAS = ((0, 1, -1, 4, -4, 5, -5, 8), (2, -2, 3, -3, 6, -6, 7, -7))
+COLUMNS = 1024
+
+
+def silu(v):
+    return v / (1.0 + jnp.exp(-v))
+
+
+def experts_kernel(
+    n_sp,
+    n_tp,
+    mix_ref,
+    send_map_ref,
+    pick_ref,
+    weight_ref,
+    out_wide_hbm,
+    out_narrow_hbm,
+    residual_hbm,
+    gain_hbm,
+    shared_gate_hbm,
+    shared_up_hbm,
+    shared_down_hbm,
+    expert_gate_hbm,
+    expert_up_hbm,
+    expert_down_hbm,
+    out_ref,
+    out_weight,
+    residual_ref,
+    gain_ref,
+    shared_in,
+    shared_down,
+    expert_gate,
+    expert_up,
+    expert_down,
+    part,
+    opposite,
+    summed,
+    landed,
+    stream,
+    gathered,
+    outgoing,
+    first_recv,
+    first_relay,
+    second_send,
+    second_recv,
+    finished,
+    back_recv,
+    back_send,
+    back_relay,
+    returned,
+    shared_send,
+    shared_recv,
+    fetch,
+    send_sems,
+    recv_sems,
+):
+    rows, depth = residual_hbm.shape
+    half = depth // 2
+    zn = n_sp // 2
+    lanes = 2 * n_tp
+    piece = outgoing.shape[1]
+    wide_rows = out_wide_hbm.shape[0]
+    ff = shared_gate_hbm.shape[1]
+    me = lax.axis_index("sp")
+    x = lax.axis_index("tp")
+    z = me // 2
+    core = lax.rem(me, 2)
+    lane = core * n_tp + x
+
+    def at_plane(delta):
+        return lax.rem(z + (delta + zn), zn)
+
+    def on_plane(delta):
+        return {"sp": at_plane(delta) * 2 + core}
+
+    def along_x(dx):
+        return {"tp": lax.rem(x + (dx + n_tp), n_tp)}
+
+    def in_plane(dc, dx):
+        other = 1 - core if dc else core
+        return {"sp": z * 2 + other, "tp": lax.rem(x + (dx + n_tp), n_tp)}
+
+    relative = [(dc, dx) for dc in range(2) for dx in range(n_tp)]
+
+    taken = [0]
+
+    def remote(source, target, place):
+        i = taken[0]
+        taken[0] += 1
+        return pltpu.make_async_remote_copy(
+            src_ref=source,
+            dst_ref=target,
+            send_sem=send_sems.at[i],
+            recv_sem=recv_sems.at[i],
+            device_id=place,
+            device_id_type=pl.DeviceIdType.MESH,
+        )
+
+    barrier = pltpu.get_barrier_semaphore()
+    greeted = [on_plane(d) for d in range(1, zn)] + [in_plane(dc, dx) for dc, dx in relative[1:]]
+    for place in greeted:
+        pl.semaphore_signal(barrier, inc=1, device_id=place, device_id_type=pl.DeviceIdType.MESH)
+
+    fetches = [
+        pltpu.make_async_copy(source, target, fetch.at[i])
+        for i, (source, target) in enumerate(
+            (
+                (out_wide_hbm, out_weight.at[pl.ds(0, wide_rows)]),
+                (out_narrow_hbm, out_weight.at[pl.ds(wide_rows, out_narrow_hbm.shape[0])]),
+                (residual_hbm, residual_ref),
+                (gain_hbm, gain_ref),
+                (shared_gate_hbm, shared_in.at[:, pl.ds(0, ff)]),
+                (shared_up_hbm, shared_in.at[:, pl.ds(ff, ff)]),
+                (shared_down_hbm, shared_down),
+                (expert_gate_hbm.at[0], expert_gate),
+                (expert_up_hbm.at[0], expert_up),
+                (expert_down_hbm.at[0], expert_down),
+            )
+        )
+    ]
+    for copy in fetches:
+        copy.start()
+
+    def chunks():
+        return [pl.ds(n, COLUMNS) for n in range(0, depth, COLUMNS)]
+
+    def project(dx):
+        q = pl.multiple_of(lax.rem(x + dx, n_tp) * rows, rows)
+        mine = mix_ref[pl.ds(q, rows), :]
+        for cols in chunks():
+            part[dx, :, cols] = jnp.dot(
+                mine, out_weight[:, cols], preferred_element_type=jnp.float32
+            ).astype(jnp.bfloat16)
+
+    lower, upper = pl.ds(0, half), pl.ds(half, half)
+    fetches[0].wait()
+    fetches[1].wait()
+    project(2)
+    pl.semaphore_wait(barrier, len(greeted))
+    over_right = remote(part.at[2, :, lower], opposite.at[0], along_x(1))
+    over_left = remote(part.at[2, :, upper], opposite.at[1], along_x(-1))
+    over_right.start()
+    over_left.start()
+    project(1)
+    straight_right = remote(part.at[1, :, upper], landed.at[0, 1], along_x(1))
+    straight_right.start()
+    project(3)
+    straight_left = remote(part.at[3, :, lower], landed.at[1, 0], along_x(-1))
+    straight_left.start()
+    project(0)
+    over_right.wait_recv()
+    summed[0] = (part[1, :, lower].astype(jnp.float32) + opposite[0].astype(jnp.float32)).astype(jnp.bfloat16)
+    joined_right = remote(summed.at[0], landed.at[0, 0], along_x(1))
+    joined_right.start()
+    over_left.wait_recv()
+    summed[1] = (part[3, :, upper].astype(jnp.float32) + opposite[1].astype(jnp.float32)).astype(jnp.bfloat16)
+    joined_left = remote(summed.at[1], landed.at[1, 1], along_x(-1))
+    joined_left.start()
+    fetches[2].wait()
+    fetches[3].wait()
+    for copy in (straight_right, straight_left, joined_right, joined_left):
+        copy.wait_recv()
+    for h, cols in enumerate((lower, upper)):
+        stream[:, cols] = (
+            residual_ref[:, cols].astype(jnp.float32)
+            + part[0, :, cols].astype(jnp.float32)
+            + landed[0, h].astype(jnp.float32)
+            + landed[1, h].astype(jnp.float32)
+        ).astype(jnp.bfloat16)
+    gathered[0] = rms_scale(stream[...].astype(jnp.float32), gain_ref[...]).astype(jnp.bfloat16)
+
+    for cols in chunks():
+        outgoing[:, :, cols] = (
+            jnp.dot(send_map_ref[...], gathered[0, :, cols], preferred_element_type=jnp.float32)
+            .astype(jnp.bfloat16)
+            .reshape(zn, piece, COLUMNS)
+        )
+    sent = [over_right, over_left, straight_right, straight_left, joined_right, joined_left]
+    far = at_plane(8)
+    relay_up = remote(outgoing.at[far, :, lower], first_relay.at[0], on_plane(4))
+    relay_down = remote(outgoing.at[far, :, upper], first_relay.at[1], on_plane(-4))
+    relay_up.start()
+    relay_down.start()
+    first = [{}, {}]
+    for ch in range(2):
+        for j, delta in enumerate(DELTAS[ch]):
+            if delta in (0, 8):
+                continue
+            first[ch][j] = remote(outgoing.at[at_plane(delta)], first_recv.at[ch, j], on_plane(delta))
+            first[ch][j].start()
+        if ch == 0:
+            spread = [remote(gathered.at[0], gathered.at[dx], along_x(dx)) for dx in (1, 3, 2)]
+            for copy in spread:
+                copy.start()
+    first_recv[0, 0] = outgoing[z]
+    far_slot = DELTAS[0].index(8)
+    onward_up = remote(first_relay.at[0], first_recv.at[0, far_slot, :, lower], on_plane(4))
+    onward_down = remote(first_relay.at[1], first_recv.at[0, far_slot, :, upper], on_plane(-4))
+    relay_up.wait_recv()
+    onward_up.start()
+    relay_down.wait_recv()
+    onward_down.start()
+    sent += [relay_up, relay_down, onward_up, onward_down] + spread
+    sent += list(first[0].values()) + list(first[1].values())
+
+    for copy in fetches[4:]:
+        copy.wait()
+    for copy in spread:
+        copy.wait_recv()
+    every = gathered[...].reshape(n_tp * rows, depth)
+    both = jnp.dot(every, shared_in[...], preferred_element_type=jnp.float32)
+    act = (silu(both[:, :ff]) * both[:, ff:]).astype(jnp.bfloat16)
+    for cols in chunks():
+        shared_send[:, :, cols] = (
+            jnp.dot(act, shared_down[:, cols], preferred_element_type=jnp.float32)
+            .astype(jnp.bfloat16)
+            .reshape(n_tp, rows, COLUMNS)
+        )
+    shared_back = [remote(shared_send.at[dx], shared_recv.at[dx - 1], along_x(-dx)) for dx in range(1, n_tp)]
+    for copy in shared_back:
+        copy.start()
+    sent += shared_back
+
+    count = lanes * piece
+    o = lax.broadcasted_iota(jnp.int32, (count, count), 0)
+    i = lax.broadcasted_iota(jnp.int32, (count, count), 1)
+    swap = jnp.where(
+        (o // piece == (i % piece) // 2) & ((o % piece) // 2 == i // piece) & (o % 2 == i % 2), 1.0, 0.0
+    ).astype(jnp.bfloat16)
+
+    def swapped(source, target, ch):
+        for cols in chunks():
+            target[ch, :, :, cols] = (
+                jnp.dot(
+                    swap, source[ch, :, :, cols].reshape(count, COLUMNS), preferred_element_type=jnp.float32
+                )
+                .astype(jnp.bfloat16)
+                .reshape(lanes, piece, COLUMNS)
+            )
+
+    def to_lanes(ch):
+        swapped(first_recv, second_send, ch)
+        copies = []
+        for r, (dc, dx) in enumerate(relative):
+            if r == 0:
+                continue
+            other = (1 - core if dc else core) * n_tp + lax.rem(x + dx, n_tp)
+            copies.append(remote(second_send.at[ch, other], second_recv.at[ch, r], in_plane(dc, dx)))
+            copies[-1].start()
+        second_recv[ch, 0] = second_send[ch, lane]
+        return copies
+
+    def run_expert(ch):
+        taken_in = second_recv[ch].reshape(count, depth)
+        gate = jnp.dot(taken_in, expert_gate[...], preferred_element_type=jnp.float32)
+        lifted = jnp.dot(taken_in, expert_up[...], preferred_element_type=jnp.float32)
+        active = (silu(gate) * lifted).astype(jnp.bfloat16)
+        for cols in chunks():
+            finished[ch, :, :, cols] = (
+                jnp.dot(active, expert_down[:, cols], preferred_element_type=jnp.float32)
+                .astype(jnp.bfloat16)
+                .reshape(lanes, piece, COLUMNS)
+            )
+        copies = []
+        for r, (dc, dx) in enumerate(relative):
+            if r == 0:
+                continue
+            copies.append(remote(finished.at[ch, r], back_recv.at[ch, lane], in_plane(dc, -dx)))
+            copies[-1].start()
+        back_recv[ch, lane] = finished[ch, 0]
+        return copies
+
+    def home(ch):
+        swapped(back_recv, back_send, ch)
+        copies = []
+        relays = []
+        for j, delta in enumerate(DELTAS[ch]):
+            if delta == 8:
+                relays = [
+                    remote(back_send.at[ch, j, :, lower], back_relay.at[0], on_plane(4)),
+                    remote(back_send.at[ch, j, :, upper], back_relay.at[1], on_plane(-4)),
+                ]
+                for copy in relays:
+                    copy.start()
+        for j, delta in enumerate(DELTAS[ch]):
+            if delta == 0:
+                returned[z] = back_send[ch, j]
+            elif delta != 8:
+                copies.append(remote(back_send.at[ch, j], returned.at[z], on_plane(-delta)))
+                copies[-1].start()
+        return copies, relays
+
+    for copy in list(first[0].values()) + [onward_up, onward_down]:
+        copy.wait_recv()
+    lane_copies = to_lanes(0)
+    for copy in lane_copies:
+        copy.wait_recv()
+    back_copies = run_expert(0)
+    for copy in back_copies:
+        copy.wait_recv()
+    home_copies, relays = home(0)
+    sent += lane_copies + back_copies + home_copies + relays
+
+    for copy in first[1].values():
+        copy.wait_recv()
+    lane_copies = to_lanes(1)
+    relays[0].wait_recv()
+    last_up = remote(back_relay.at[0], returned.at[at_plane(-4), :, lower], on_plane(4))
+    last_up.start()
+    relays[1].wait_recv()
+    last_down = remote(back_relay.at[1], returned.at[at_plane(4), :, upper], on_plane(-4))
+    last_down.start()
+    for copy in lane_copies:
+        copy.wait_recv()
+    back_copies = run_expert(1)
+    for copy in back_copies:
+        copy.wait_recv()
+    more_home, _ = home(1)
+    sent += lane_copies + back_copies + more_home + [last_up, last_down]
+
+    for copy in shared_back:
+        copy.wait_recv()
+    for copy in home_copies + more_home + [last_up, last_down]:
+        copy.wait_recv()
+    for cols in chunks():
+        total = stream[:, cols].astype(jnp.float32) + shared_send[0, :, cols].astype(jnp.float32)
+        for dx in range(n_tp - 1):
+            total = total + shared_recv[dx, :, cols].astype(jnp.float32)
+        results = returned[:, :, cols].reshape(zn * piece, COLUMNS)
+        for c in range(pick_ref.shape[0]):
+            total = total + weight_ref[:, c : c + 1] * jnp.dot(
+                pick_ref[c], results, preferred_element_type=jnp.float32
+            )
+        out_ref[:, cols] = total.astype(out_ref.dtype)
+    for copy in sent:
+        copy.wait_send()
+
+
+def projected_experts(
+    mix,
+    send_map,
+    pick,
+    route_weights,
+    out_wide,
+    out_narrow,
+    residual,
+    gain,
+    shared_gate,
+    shared_up,
+    shared_down,
+    expert_gate,
+    expert_up,
+    expert_down,
+):
+    rows, depth = residual.shape
+    n_sp, n_tp = lax.axis_size("sp"), lax.axis_size("tp")
+    zn, lanes = n_sp // 2, 2 * n_tp
+    piece = send_map.shape[0] // zn
+    ff = shared_gate.shape[1]
+    assert zn == 16 and n_tp == 4 and piece == 2 * lanes and expert_gate.shape[0] == 1
+    vmem, hbm = pl.BlockSpec(memory_space=pltpu.VMEM), pl.BlockSpec(memory_space=pltpu.HBM)
+    bf16 = jnp.bfloat16
+    chunk = (2, lanes, piece, depth)
+    dma = pltpu.SemaphoreType.DMA
+    return pl.pallas_call(
+        functools.partial(experts_kernel, n_sp, n_tp),
+        out_shape=jax.ShapeDtypeStruct((rows, depth), bf16),
+        in_specs=[vmem] * 4 + [hbm] * 10,
+        out_specs=vmem,
+        scratch_shapes=[
+            pltpu.VMEM((out_wide.shape[0] + out_narrow.shape[0], depth), bf16),
+            pltpu.VMEM((rows, depth), bf16),
+            pltpu.VMEM((1, depth), jnp.float32),
+            pltpu.VMEM((depth, 2 * ff), bf16),
+            pltpu.VMEM(shared_down.shape, bf16),
+            pltpu.VMEM(expert_gate.shape[1:], bf16),
+            pltpu.VMEM(expert_up.shape[1:], bf16),
+            pltpu.VMEM(expert_down.shape[1:], bf16),
+            pltpu.VMEM((n_tp, rows, depth), bf16),
+            pltpu.VMEM((2, rows, depth // 2), bf16),
+            pltpu.VMEM((2, rows, depth // 2), bf16),
+            pltpu.VMEM((2, 2, rows, depth // 2), bf16),
+            pltpu.VMEM((rows, depth), bf16),
+            pltpu.VMEM((n_tp, rows, depth), bf16),
+            pltpu.VMEM((zn, piece, depth), bf16),
+            pltpu.VMEM(chunk, bf16),
+            pltpu.VMEM((2, piece, depth // 2), bf16),
+            pltpu.VMEM(chunk, bf16),
+            pltpu.VMEM(chunk, bf16),
+            pltpu.VMEM(chunk, bf16),
+            pltpu.VMEM(chunk, bf16),
+            pltpu.VMEM(chunk, bf16),
+            pltpu.VMEM((2, piece, depth // 2), bf16),
+            pltpu.VMEM((zn, piece, depth), bf16),
+            pltpu.VMEM((n_tp, rows, depth), bf16),
+            pltpu.VMEM((n_tp - 1, rows, depth), bf16),
+            dma((10,)),
+            dma((80,)),
+            dma((80,)),
+        ],
+        compiler_params=pltpu.CompilerParams(
+            collective_id=1, has_side_effects=True, vmem_limit_bytes=56 * 1024 * 1024
+        ),
+    )(
+        mix,
+        send_map,
+        pick,
+        route_weights,
+        out_wide,
+        out_narrow,
+        residual,
+        gain.reshape(1, depth),
+        shared_gate,
+        shared_up,
+        shared_down,
+        expert_gate,
+        expert_up,
+        expert_down,
     )
 
 
@@ -397,31 +853,10 @@
         narrow_value_weight,
         latent_norm_scale,
     )
-    wide_cols = out_wide.shape[0]
-    wide_mix, narrow_mix = mix[:, :wide_cols], mix[:, wide_cols:]
-    projected = summed_on_arrival(
-        (
-            jnp.dot(wide_mix, out_wide, preferred_element_type=jnp.float32)
-            + jnp.dot(narrow_mix, out_narrow, preferred_element_type=jnp.float32)
-        ).astype(jnp.bfloat16),
-        "tp",
-        0,
-    )
-    stream = (residual.astype(jnp.float32) + projected).astype(jnp.bfloat16)
-    normed = rms_scale(stream.astype(jnp.float32), ffn_gain).astype(jnp.bfloat16)
-    piece = lax.all_gather(normed, "tp", axis=0, tiled=True)
-    gate_part = jnp.dot(piece, shared_gate, preferred_element_type=jnp.float32)
-    up_part = jnp.dot(piece, shared_up, preferred_element_type=jnp.float32)
-    active = (jax.nn.silu(gate_part) * up_part).astype(jnp.bfloat16)
-    shared_terms = jnp.dot(active, shared_down, preferred_element_type=jnp.float32)
-    shared = lax.psum_scatter(
-        shared_terms.astype(jnp.bfloat16), "tp", scatter_dimension=0, tiled=True
-    ).astype(jnp.float32)
     rows_here, top_count = routes.shape
     local_experts = expert_gate.shape[0]
     experts_all = local_experts * lax.axis_size(("sp", "tp"))
     capacity = max(2, 2 * top_count * rows_here // experts_all)
-    model_width = normed.shape[1]
     flat_routes = routes.reshape(-1)
     assigned = flat_routes.shape[0]
     choose = (flat_routes[:, None] == jnp.arange(experts_all, dtype=jnp.int32)[None, :]).astype(
@@ -436,32 +871,25 @@
         == jnp.arange(experts_all * capacity, dtype=jnp.int32)[:, None, None],
         axis=2,
     ).astype(jnp.bfloat16)
-    outgoing = jnp.dot(send_map, normed, preferred_element_type=jnp.float32).astype(jnp.bfloat16)
-    incoming = lax.all_to_all(outgoing, ("sp", "tp"), split_axis=0, concat_axis=0, tiled=True)
-    finished = []
-    for x in range(local_experts):
-        rows = incoming
-        if local_experts > 1:
-            rows = incoming.reshape(-1, local_experts, capacity, model_width)[:, x].reshape(-1, model_width)
-        gate_part = jnp.dot(rows, expert_gate[x], preferred_element_type=jnp.float32)
-        up_part = jnp.dot(rows, expert_up[x], preferred_element_type=jnp.float32)
-        active = (jax.nn.silu(gate_part) * up_part).astype(jnp.bfloat16)
-        finished.append(
-            jnp.dot(active, expert_down[x], preferred_element_type=jnp.float32).astype(jnp.bfloat16)
-        )
-    if local_experts > 1:
-        stacked = jnp.stack([f.reshape(-1, capacity, model_width) for f in finished], axis=1)
-        finished = [stacked.reshape(-1, model_width)]
-    returned = lax.all_to_all(finished[0], ("sp", "tp"), split_axis=0, concat_axis=0, tiled=True)
     chosen = target.reshape(rows_here, top_count)
-    places = jnp.arange(experts_all * capacity, dtype=jnp.int32)[None, :]
-    routed = jnp.zeros((rows_here, model_width), jnp.float32)
-    for c in range(top_count):
-        pick = (chosen[:, c : c + 1] == places).astype(jnp.bfloat16)
-        routed = routed + route_weights[:, c : c + 1] * jnp.dot(
-            pick, returned, preferred_element_type=jnp.float32
-        )
-    return (stream.astype(jnp.float32) + shared + routed).astype(jnp.bfloat16)
+    places = jnp.arange(experts_all * capacity, dtype=jnp.int32)
+    pick = (chosen.T[:, :, None] == places[None, None, :]).astype(jnp.bfloat16)
+    return projected_experts(
+        mix,
+        send_map,
+        pick,
+        route_weights,
+        out_wide,
+        out_narrow,
+        residual,
+        ffn_gain,
+        shared_gate,
+        shared_up,
+        shared_down,
+        expert_gate,
+        expert_up,
+        expert_down,
+    )
 
 
 def solution(mesh):

time: 389 us -> 341 us (0.88)
  Pallas kernels: 52 us -> 316 us
  blocking collectives: 134 us -> 0 us
  waiting for transfers between devices: 110 us -> 0 us
  matrix products: 28.3 us -> 0.19 us
  starting transfers between devices: 15.7 us -> 0 us
  between operations: 13.6 us -> 0.08 us
  local copies, waits for them, and re-layouts: 29.6 us -> 21.9 us
    pallas_call x0 -> x1, Pallas kernels: none -> 262 us  [projected_experts(): pl.pallas_call(functools.partial(experts_kernel, n_sp, n_tp), out_shape=j...]
    all_to_all x1 -> x0, blocking collectives: 134 us -> none  [body(): lax.all_to_all(outgoing, ('sp', 'tp'), split_axis=0, concat_axis=0, tiled...]
    all_to_all x2 -> x0, waiting for transfers between devices: 64.6 us -> none  [the longest x1 43 us: body(): lax.all_to_all(finished[0], ('sp', 'tp'), split_axis=0, concat_axis=0, ti...]
    all_gather x1 -> x0, waiting for transfers between devices: 44.9 us -> none  [body(): piece = lax.all_gather(normed, 'tp', axis=0, tiled=True)]
    dot_general x9 -> x0, matrix products: 28.1 us -> none  [the longest x2 6.5 us: body(): jnp.dot(pick, returned, preferred_element_type=jnp.float32)]
    all_to_all x4 -> x0, local copies, waits for them, and re-layouts: 17.1 us -> none  [the longest x2 8.55 us: body(): lax.all_to_all(finished[0], ('sp', 'tp'), split_axis=0, concat_axis=0, ti...]
    all_to_all x2 -> x0, starting transfers between devices: 15.6 us -> none  [the longest x1 10.9 us: body(): lax.all_to_all(finished[0], ('sp', 'tp'), split_axis=0, concat_axis=0, ti...]
    unnamed x40 -> x36, local copies, waits for them, and re-layouts: 12.2 us -> 20.8 us
  transfers between devices with their start and end apart: 4 -> 0, of which waited for: 3 -> 0; matrix products, arithmetic and copies ran while one was open for 3% -> 0% of each run, Pallas kernels for 0% -> 0%
where the time goes in v2:
time: 341 us; the launch traced here: 339 us
  Pallas kernels  316 us (93%)
  local copies, waits for them, and re-layouts  21.9 us (6%)
    pallas_call x1, Pallas kernels, projected_experts(): pl.pallas_call(functools.partial(experts_kernel, n_sp, n_tp), out_shape=j...  262 us
    pallas_call x1, Pallas kernels, attention(): pl.pallas_call(functools.partial(attention_kernel, n_sp, n_tp), out_shape...  53.1 us
    unnamed x36, local copies, waits for them, and re-layouts  20.8 us

profile of v2, /device:TPU:35, one launch (start us, length us, event | category | flops | bytes accessed | tf_op | source)
XLA Modules:
  0.0 339.2 jit_solution(10054373235241190423)
XLA Ops:
  0.0 1.4 copy.56.weight_ref
  1.4 0.8 copy.53
  2.1 0.1 eq.18
  2.3 0.2 fusion
  2.5 0.1 convert_element_type.18
  2.6 0.1 copy.54
  2.7 0.7 multiply_add_fusion
  3.4 0.1 fusion.1
  3.5 0.7 copy.55.send_map_ref
  4.2 0.7 fusion.2.pick_ref
  4.9 0.9 copy.52.rope_key_hbm
  5.8 0.0 copy-start.1
  5.8 0.9 copy-done.1
  6.8 0.9 copy-done.2
  7.7 0.9 copy-done.3
  8.7 0.9 copy-done.4
  9.6 0.9 copy-done.5
  10.5 0.9 copy-done.6
  11.4 0.9 copy-done.7
  12.3 0.9 copy-done.8
  13.2 0.9 copy-done.9
  14.1 0.7 copy-done.10
  14.8 0.7 copy-done.11
  15.5 0.7 copy-done.12
  16.2 53.1 %shard_map.235.mix_ref = bf16[256,384]{1,0:T(8,128)(2,1)S(1)} custom-call(bf16[256,512]{1,0:T(8,128)(2,1)S(1)} %copy-done.1, bf16[256,64]{1,0:T(8,128)(2,1)S(1)} %copy.52.rope_key_hbm, bf16[256,384]{1,0:T(8,128)(2,1)S(1)} %copy-done.4, bf16[256,256]{1,0:T(8,128)(2,1)S(1)} %copy-done.5, bf16[512,256]{1,0:T(8,128)(2,1)S(1)} %copy-done.2, ...), custom_call_target="tpu_custom_call" | custom-call | tf_op jit(solution)/shard_map/pallas_call | solution.py:351
  69.3 0.0 copy-start
  69.3 0.7 copy-done
  70.0 0.0 copy-done.13
  70.0 2.4 copy.57.expert_gate_hbm
  72.4 2.4 copy.58.expert_up_hbm
  74.9 262.4 %shard_map.236 = bf16[64,4096]{1,0:T(8,128)(2,1)} custom-call(bf16[256,384]{1,0:T(8,128)(2,1)} %copy-done, bf16[256,64]{1,0:T(8,128)(2,1)} %copy.55.send_map_ref, bf16[2,64,256]{2,1,0:T(8,128)(2,1)} %fusion.2.pick_ref, f32[64,2]{1,0:T(8,128)} %copy.56.weight_ref, bf16[256,4096]{1,0:T(8,128)(2,1)} %out_wide_hbm.1, bf16[128,4096]{1,0:T(8,128)(2,1)} %out_narrow_hbm.1, ...), custom_call_target="tpu_custom_call" | custom-call | tf_op jit(solution)/shard_map/pallas_call | solution.py:765
  337.3 1.9 copy.60
  (16 shorter events, 0.0 us)
Async XLA Ops:
  5.8 1.0 copy-start.1
  6.8 0.9 copy-start.2
  7.7 0.9 copy-start.3
  8.7 0.9 copy-start.4
  9.6 0.9 copy-start.5
  10.5 0.9 copy-start.6
  11.4 0.9 copy-start.7
  12.3 0.9 copy-start.8
  13.2 0.9 copy-start.9
  14.1 0.7 copy-start.10
  14.8 0.7 copy-start.11
  15.5 0.7 copy-start.12
  16.2 53.8 %copy-start.13 = (bf16[1,4096,192]{1,2,0:T(8,128)(2,1)S(1)}, bf16[1,4096,192]{1,2,0:T(8,128)(2,1)}, u32[]{:S(2)}) copy-start(bf16[1,4096,192]{1,2,0:T(8,128)(2,1)} %param.41) | copy-start | bytes 4718596
  69.3 0.7 copy-start
  70.0 2.4 copy-start.14

commit v3 on v2

--- a/solution.py
+++ b/solution.py
@@ -12,6 +12,7 @@
 WIDE_HEAD_SIZE = 128
 NARROW_HEAD_SIZE = 64
 LANES = 128
+VMEM_BYTES = 67_043_328
 
 
 EPS = 1e-06
@@ -135,7 +136,7 @@
 
     lat = latent_ref[...].astype(jnp.float32)
     normed = rms_scale(lat, gain_ref[...]).astype(jnp.bfloat16)
-    rope = rope_key_ref[...].astype(jnp.float32)
+    rope = rope_key_ref[...].astype(jnp.float32).T
     turned = turn(jnp.concatenate([rope, jnp.zeros_like(rope)], axis=1))
     for q in range(n_tp):
         rows_buf[me, q, :, :width] = normed[q * quarter : (q + 1) * quarter]
@@ -355,7 +356,7 @@
         out_specs=vmem,
         scratch_shapes=[
             pltpu.VMEM(latent.shape, jnp.bfloat16),
-            pltpu.VMEM(rope_key.shape, jnp.bfloat16),
+            pltpu.VMEM(rope_key.shape[::-1], jnp.bfloat16),
             pltpu.VMEM(wide_query.shape, jnp.bfloat16),
             pltpu.VMEM(narrow_query.shape, jnp.bfloat16),
             pltpu.VMEM(wide_key.shape, jnp.bfloat16),
@@ -379,11 +380,11 @@
             dma((2, hops)),
         ],
         compiler_params=pltpu.CompilerParams(
-            collective_id=0, has_side_effects=True, vmem_limit_bytes=48 * 1024 * 1024
+            collective_id=0, has_side_effects=True, vmem_limit_bytes=VMEM_BYTES
         ),
     )(
         latent,
-        rope_key,
+        rope_key.T,
         wide_query,
         narrow_query,
         wide_key,
@@ -400,6 +401,7 @@
 
 DELTAS = ((0, 1, -1, 4, -4, 5, -5, 8), (2, -2, 3, -3, 6, -6, 7, -7))
 COLUMNS = 1024
+CAPACITY = 2
 
 
 def silu(v):
@@ -410,9 +412,8 @@
     n_sp,
     n_tp,
     mix_ref,
-    send_map_ref,
-    pick_ref,
-    weight_ref,
+    routes_hbm,
+    weight_hbm,
     out_wide_hbm,
     out_narrow_hbm,
     residual_hbm,
@@ -424,13 +425,15 @@
     expert_up_hbm,
     expert_down_hbm,
     out_ref,
+    routes_ref,
+    weight_ref,
+    places,
     out_weight,
     residual_ref,
     gain_ref,
     shared_in,
     shared_down,
-    expert_gate,
-    expert_up,
+    expert_in,
     expert_down,
     part,
     opposite,
@@ -461,6 +464,8 @@
     piece = outgoing.shape[1]
     wide_rows = out_wide_hbm.shape[0]
     ff = shared_gate_hbm.shape[1]
+    hidden = expert_gate_hbm.shape[1]
+    top_count = routes_hbm.shape[0]
     me = lax.axis_index("sp")
     x = lax.axis_index("tp")
     z = me // 2
@@ -505,6 +510,8 @@
         pltpu.make_async_copy(source, target, fetch.at[i])
         for i, (source, target) in enumerate(
             (
+                (routes_hbm, routes_ref),
+                (weight_hbm, weight_ref),
                 (out_wide_hbm, out_weight.at[pl.ds(0, wide_rows)]),
                 (out_narrow_hbm, out_weight.at[pl.ds(wide_rows, out_narrow_hbm.shape[0])]),
                 (residual_hbm, residual_ref),
@@ -512,8 +519,8 @@
                 (shared_gate_hbm, shared_in.at[:, pl.ds(0, ff)]),
                 (shared_up_hbm, shared_in.at[:, pl.ds(ff, ff)]),
                 (shared_down_hbm, shared_down),
-                (expert_gate_hbm.at[0], expert_gate),
-                (expert_up_hbm.at[0], expert_up),
+                (expert_gate_hbm.at[0], expert_in.at[pl.ds(0, hidden)]),
+                (expert_up_hbm.at[0], expert_in.at[pl.ds(hidden, hidden)]),
                 (expert_down_hbm.at[0], expert_down),
             )
         )
@@ -533,8 +540,8 @@
             ).astype(jnp.bfloat16)
 
     lower, upper = pl.ds(0, half), pl.ds(half, half)
-    fetches[0].wait()
-    fetches[1].wait()
+    for copy in fetches[:4]:
+        copy.wait()
     project(2)
     pl.semaphore_wait(barrier, len(greeted))
     over_right = remote(part.at[2, :, lower], opposite.at[0], along_x(1))
@@ -548,6 +555,26 @@
     straight_left = remote(part.at[3, :, lower], landed.at[1, 0], along_x(-1))
     straight_left.start()
     project(0)
+
+    r0 = lax.broadcasted_iota(jnp.int32, (rows, rows), 0)
+    r1 = lax.broadcasted_iota(jnp.int32, (rows, rows), 1)
+
+    def upright(row):
+        return jnp.sum(jnp.where(r0 == r1, row, 0.0), axis=1, keepdims=True)
+
+    named = [routes_ref[c : c + 1, :].astype(jnp.float32) for c in range(top_count)]
+    shares = [upright(weight_ref[c : c + 1, :]) for c in range(top_count)]
+    slot = lax.broadcasted_iota(jnp.int32, (zn * piece, rows), 0).astype(jnp.float32)
+    maps = []
+    for c in range(top_count):
+        earlier = jnp.zeros((1, rows), jnp.float32)
+        for other in range(top_count):
+            same = (upright(named[other]) == named[c]) & (r0 < r1)
+            earlier = earlier + jnp.sum(jnp.where(same, 1.0, 0.0), axis=0, keepdims=True)
+        maps.append(jnp.where(slot == named[c] * CAPACITY + earlier, 1.0, 0.0))
+        places[c] = maps[c].T.astype(jnp.bfloat16)
+    send_map = sum(maps[1:], maps[0]).astype(jnp.bfloat16)
+
     over_right.wait_recv()
     summed[0] = (part[1, :, lower].astype(jnp.float32) + opposite[0].astype(jnp.float32)).astype(jnp.bfloat16)
     joined_right = remote(summed.at[0], landed.at[0, 0], along_x(1))
@@ -556,8 +583,8 @@
     summed[1] = (part[3, :, upper].astype(jnp.float32) + opposite[1].astype(jnp.float32)).astype(jnp.bfloat16)
     joined_left = remote(summed.at[1], landed.at[1, 1], along_x(-1))
     joined_left.start()
-    fetches[2].wait()
-    fetches[3].wait()
+    fetches[4].wait()
+    fetches[5].wait()
     for copy in (straight_right, straight_left, joined_right, joined_left):
         copy.wait_recv()
     for h, cols in enumerate((lower, upper)):
@@ -571,7 +598,7 @@
 
     for cols in chunks():
         outgoing[:, :, cols] = (
-            jnp.dot(send_map_ref[...], gathered[0, :, cols], preferred_element_type=jnp.float32)
+            jnp.dot(send_map, gathered[0, :, cols], preferred_element_type=jnp.float32)
             .astype(jnp.bfloat16)
             .reshape(zn, piece, COLUMNS)
         )
@@ -603,7 +630,7 @@
     sent += [relay_up, relay_down, onward_up, onward_down] + spread
     sent += list(first[0].values()) + list(first[1].values())
 
-    for copy in fetches[4:]:
+    for copy in fetches[6:]:
         copy.wait()
     for copy in spread:
         copy.wait_recv()
@@ -652,8 +679,15 @@
 
     def run_expert(ch):
         taken_in = second_recv[ch].reshape(count, depth)
-        gate = jnp.dot(taken_in, expert_gate[...], preferred_element_type=jnp.float32)
-        lifted = jnp.dot(taken_in, expert_up[...], preferred_element_type=jnp.float32)
+        gate, lifted = (
+            lax.dot_general(
+                taken_in,
+                expert_in[pl.ds(at, hidden), :],
+                (((1,), (1,)), ((), ())),
+                preferred_element_type=jnp.float32,
+            )
+            for at in (0, hidden)
+        )
         active = (silu(gate) * lifted).astype(jnp.bfloat16)
         for cols in chunks():
             finished[ch, :, :, cols] = (
@@ -727,10 +761,8 @@
         for dx in range(n_tp - 1):
             total = total + shared_recv[dx, :, cols].astype(jnp.float32)
         results = returned[:, :, cols].reshape(zn * piece, COLUMNS)
-        for c in range(pick_ref.shape[0]):
-            total = total + weight_ref[:, c : c + 1] * jnp.dot(
-                pick_ref[c], results, preferred_element_type=jnp.float32
-            )
+        for c in range(top_count):
+            total = total + shares[c] * jnp.dot(places[c], results, preferred_element_type=jnp.float32)
         out_ref[:, cols] = total.astype(out_ref.dtype)
     for copy in sent:
         copy.wait_send()
@@ -738,8 +770,7 @@
 
 def projected_experts(
     mix,
-    send_map,
-    pick,
+    routes,
     route_weights,
     out_wide,
     out_narrow,
@@ -755,9 +786,10 @@
     rows, depth = residual.shape
     n_sp, n_tp = lax.axis_size("sp"), lax.axis_size("tp")
     zn, lanes = n_sp // 2, 2 * n_tp
-    piece = send_map.shape[0] // zn
+    piece = CAPACITY * lanes
     ff = shared_gate.shape[1]
-    assert zn == 16 and n_tp == 4 and piece == 2 * lanes and expert_gate.shape[0] == 1
+    hidden = expert_gate.shape[2]
+    assert zn == 16 and n_tp == 4 and expert_gate.shape[0] == 1
     vmem, hbm = pl.BlockSpec(memory_space=pltpu.VMEM), pl.BlockSpec(memory_space=pltpu.HBM)
     bf16 = jnp.bfloat16
     chunk = (2, lanes, piece, depth)
@@ -765,16 +797,18 @@
     return pl.pallas_call(
         functools.partial(experts_kernel, n_sp, n_tp),
         out_shape=jax.ShapeDtypeStruct((rows, depth), bf16),
-        in_specs=[vmem] * 4 + [hbm] * 10,
+        in_specs=[vmem] + [hbm] * 12,
         out_specs=vmem,
         scratch_shapes=[
+            pltpu.VMEM(routes.shape[::-1], jnp.int32),
+            pltpu.VMEM(route_weights.shape[::-1], jnp.float32),
+            pltpu.VMEM((routes.shape[1], rows, zn * piece), bf16),
             pltpu.VMEM((out_wide.shape[0] + out_narrow.shape[0], depth), bf16),
             pltpu.VMEM((rows, depth), bf16),
             pltpu.VMEM((1, depth), jnp.float32),
             pltpu.VMEM((depth, 2 * ff), bf16),
             pltpu.VMEM(shared_down.shape, bf16),
-            pltpu.VMEM(expert_gate.shape[1:], bf16),
-            pltpu.VMEM(expert_up.shape[1:], bf16),
+            pltpu.VMEM((2 * hidden, depth), bf16),
             pltpu.VMEM(expert_down.shape[1:], bf16),
             pltpu.VMEM((n_tp, rows, depth), bf16),
             pltpu.VMEM((2, rows, depth // 2), bf16),
@@ -794,18 +828,17 @@
             pltpu.VMEM((zn, piece, depth), bf16),
             pltpu.VMEM((n_tp, rows, depth), bf16),
             pltpu.VMEM((n_tp - 1, rows, depth), bf16),
-            dma((10,)),
+            dma((12,)),
             dma((80,)),
             dma((80,)),
         ],
         compiler_params=pltpu.CompilerParams(
-            collective_id=1, has_side_effects=True, vmem_limit_bytes=56 * 1024 * 1024
+            collective_id=1, has_side_effects=True, vmem_limit_bytes=VMEM_BYTES
         ),
     )(
         mix,
-        send_map,
-        pick,
-        route_weights,
+        routes.T,
+        route_weights.T,
         out_wide,
         out_narrow,
         residual,
@@ -813,8 +846,8 @@
         shared_gate,
         shared_up,
         shared_down,
-        expert_gate,
-        expert_up,
+        jnp.swapaxes(expert_gate, 1, 2),
+        jnp.swapaxes(expert_up, 1, 2),
         expert_down,
     )
 
@@ -853,31 +886,9 @@
         narrow_value_weight,
         latent_norm_scale,
     )
-    rows_here, top_count = routes.shape
-    local_experts = expert_gate.shape[0]
-    experts_all = local_experts * lax.axis_size(("sp", "tp"))
-    capacity = max(2, 2 * top_count * rows_here // experts_all)
-    flat_routes = routes.reshape(-1)
-    assigned = flat_routes.shape[0]
-    choose = (flat_routes[:, None] == jnp.arange(experts_all, dtype=jnp.int32)[None, :]).astype(
-        jnp.float32
-    )
-    lower_mask = (jnp.arange(assigned)[:, None] > jnp.arange(assigned)[None, :]).astype(jnp.float32)
-    earlier = jnp.dot(lower_mask, choose, precision=lax.Precision.HIGHEST)
-    slots = jnp.sum(earlier * choose, axis=1).astype(jnp.int32)
-    target = flat_routes * capacity + slots
-    send_map = jnp.any(
-        target.reshape(rows_here, top_count)[None, :, :]
-        == jnp.arange(experts_all * capacity, dtype=jnp.int32)[:, None, None],
-        axis=2,
-    ).astype(jnp.bfloat16)
-    chosen = target.reshape(rows_here, top_count)
-    places = jnp.arange(experts_all * capacity, dtype=jnp.int32)
-    pick = (chosen.T[:, :, None] == places[None, None, :]).astype(jnp.bfloat16)
     return projected_experts(
         mix,
-        send_map,
-        pick,
+        routes,
         route_weights,
         out_wide,
         out_narrow,

time: 341 us -> 320 us (0.938)
  local copies, waits for them, and re-layouts: 21.9 us -> 1.87 us
    unnamed x36 -> x1, local copies, waits for them, and re-layouts: 20.8 us -> 1.87 us
where the time goes in v3:
time: 320 us
  Pallas kernels  318 us (99%)
    pallas_call x1, Pallas kernels, projected_experts(): pl.pallas_call(functools.partial(experts_kernel, n_sp, n_tp), out_shape=j...  265 us
    pallas_call x1, Pallas kernels, attention(): pl.pallas_call(functools.partial(attention_kernel, n_sp, n_tp), out_shape...  52.8 us

profile of v3, /device:TPU:35, one launch (start us, length us, event | category | flops | bytes accessed | tf_op | source)
XLA Modules:
  0.0 319.9 jit_solution(1985123482780864739)
XLA Ops:
  0.0 52.8 %shard_map.235.mix_ref = bf16[256,384]{1,0:T(8,128)(2,1)} custom-call(bf16[256,512]{1,0:T(8,128)(2,1)} %latent_hbm.1, bf16[64,256]{1,0:T(8,128)(2,1)} %bitcast.9, bf16[256,384]{1,0:T(8,128)(2,1)} %wide_query_hbm.1, bf16[256,256]{1,0:T(8,128)(2,1)} %narrow_query_hbm.1, bf16[512,256]{1,0:T(8,128)(2,1)} %wide_key_hbm.1, bf16[512,256]{1,0:T(8,128)(2,1)} %wide_value_hbm.1, ...), custom_call_target="tpu_custom_call" | custom-call | tf_op jit(solution)/shard_map/pallas_call | solution.py:352
  52.8 265.2 %shard_map.236 = bf16[64,4096]{1,0:T(8,128)(2,1)} custom-call(bf16[256,384]{1,0:T(8,128)(2,1)} %shard_map.235.mix_ref, s32[2,64]{1,0:T(2,128)} %bitcast.12, f32[2,64]{1,0:T(2,128)} %bitcast.13, bf16[256,4096]{1,0:T(8,128)(2,1)} %out_wide_hbm.1, bf16[128,4096]{1,0:T(8,128)(2,1)} %out_narrow_hbm.1, bf16[64,4096]{1,0:T(8,128)(2,1)} %residual_hbm.1, ...), custom_call_target="tpu_custom_call" | custom-call | tf_op jit(solution)/shard_map/pallas_call | solution.py:797
  318.0 1.9 copy.27

commit v4 on v3

--- a/solution.py
+++ b/solution.py
@@ -182,7 +182,7 @@
             dst_ref=spot,
             send_sem=x_send.at[d, k, j],
             recv_sem=x_recv.at[d, k, j],
-            device_id={"tp": right if j == 0 else left},
+            device_id={"tp": jnp.where(j == 0, right, left)},
             device_id_type=pl.DeviceIdType.MESH,
         )
 
@@ -267,42 +267,38 @@
     attend(z, True)
 
     def one_step(k, carry):
-        def forward(d, c):
-            @pl.when(arrives(d, k))
+        def quarter_step(j, carry):
+            def forward(d, c):
+                @pl.when(arrives(d, k))
+                def _():
+                    along_z(d, k - 1, j).wait_recv()
+
+                @pl.when(goes_on(d, k))
+                def _():
+                    along_z(d, k, j).start()
+
+                @pl.when(seen(d, k))
+                def _():
+                    along_x(d, k, j).start()
+
+                @pl.when(seen(d, k - 1) & (j == 0))
+                def _():
+                    for side in range(2):
+                        along_x(d, k - 1, side).wait_recv()
+                    to_partner(d, k - 1).start()
+
+                return c
+
+            lax.fori_loop(0, 2, forward, 0)
+
+            @pl.when(seen(j, k - 2))
             def _():
-                for j in range(2):
-                    along_z(d, k - 1, j).wait_recv()
-
-            @pl.when(goes_on(d, k))
-            def _():
-                for j in range(2):
-                    along_z(d, k, j).start()
-
-            @pl.when(seen(d, k))
-            def _():
-                for j in range(2):
-                    along_x(d, k, j).start()
-
-            @pl.when(seen(d, k - 1))
-            def _():
-                for j in range(2):
-                    along_x(d, k - 1, j).wait_recv()
-                to_partner(d, k - 1).start()
-
-            return c
-
-        lax.fori_loop(0, 2, forward, 0)
-
-        def work(d, c):
-            @pl.when(seen(d, k - 2))
-            def _():
-                to_partner(d, k - 2).wait_recv()
-                attend(jnp.where(d == 0, z - k + 2, z + k - 2 - zn), False)
-
-            return c
-
-        lax.fori_loop(0, 2, work, 0)
-        return carry
+                to_partner(j, k - 2).wait_recv()
+                attend(jnp.where(j == 0, z - k + 2, z + k - 2 - zn), False)
+
+            return carry
+
+        return lax.fori_loop(0, 2, quarter_step, carry)
 
     lax.fori_loop(1, steps_up + 3, one_step, 0)
 
@@ -399,7 +395,7 @@
     )
 
 
-DELTAS = ((0, 1, -1, 4, -4, 5, -5, 8), (2, -2, 3, -3, 6, -6, 7, -7))
+DELTAS = ((0, 8, 7, -7, 4, -4, 1, -1), (6, -6, 5, -5, 3, -3, 2, -2))
 COLUMNS = 1024
 CAPACITY = 2
 
@@ -630,24 +626,6 @@
     sent += [relay_up, relay_down, onward_up, onward_down] + spread
     sent += list(first[0].values()) + list(first[1].values())
 
-    for copy in fetches[6:]:
-        copy.wait()
-    for copy in spread:
-        copy.wait_recv()
-    every = gathered[...].reshape(n_tp * rows, depth)
-    both = jnp.dot(every, shared_in[...], preferred_element_type=jnp.float32)
-    act = (silu(both[:, :ff]) * both[:, ff:]).astype(jnp.bfloat16)
-    for cols in chunks():
-        shared_send[:, :, cols] = (
-            jnp.dot(act, shared_down[:, cols], preferred_element_type=jnp.float32)
-            .astype(jnp.bfloat16)
-            .reshape(n_tp, rows, COLUMNS)
-        )
-    shared_back = [remote(shared_send.at[dx], shared_recv.at[dx - 1], along_x(-dx)) for dx in range(1, n_tp)]
-    for copy in shared_back:
-        copy.start()
-    sent += shared_back
-
     count = lanes * piece
     o = lax.broadcasted_iota(jnp.int32, (count, count), 0)
     i = lax.broadcasted_iota(jnp.int32, (count, count), 1)
@@ -727,6 +705,21 @@
     for copy in list(first[0].values()) + [onward_up, onward_down]:
         copy.wait_recv()
     lane_copies = to_lanes(0)
+
+    for copy in fetches[6:]:
+        copy.wait()
+    for copy in spread:
+        copy.wait_recv()
+    every = gathered[...].reshape(n_tp * rows, depth)
+    both = jnp.dot(every, shared_in[...], preferred_element_type=jnp.float32)
+    act = (silu(both[:, :ff]) * both[:, ff:]).astype(jnp.bfloat16)
+    for cols in chunks():
+        shared_send[:, :, cols] = (
+            jnp.dot(act, shared_down[:, cols], preferred_element_type=jnp.float32)
+            .astype(jnp.bfloat16)
+            .reshape(n_tp, rows, COLUMNS)
+        )
+
     for copy in lane_copies:
         copy.wait_recv()
     back_copies = run_expert(0)
@@ -747,6 +740,10 @@
     for copy in lane_copies:
         copy.wait_recv()
     back_copies = run_expert(1)
+    shared_back = [remote(shared_send.at[dx], shared_recv.at[dx - 1], along_x(-dx)) for dx in range(1, n_tp)]
+    for copy in shared_back:
+        copy.start()
+    sent += shared_back
     for copy in back_copies:
         copy.wait_recv()
     more_home, _ = home(1)

time: 320 us -> 320 us (level)
    pallas_call x1, Pallas kernels: 52.8 us -> 49.4 us  [attention(): pl.pallas_call(functools.partial(attention_kernel, n_sp, n_tp), out_shape...]
where the time goes in v4:
time: 320 us
  Pallas kernels  318 us (99%)
    pallas_call x1, Pallas kernels, projected_experts(): pl.pallas_call(functools.partial(experts_kernel, n_sp, n_tp), out_shape=j...  268 us
    pallas_call x1, Pallas kernels, attention(): pl.pallas_call(functools.partial(attention_kernel, n_sp, n_tp), out_shape...  49.4 us

profile of v4, /device:TPU:35, one launch (start us, length us, event | category | flops | bytes accessed | tf_op | source)
XLA Modules:
  0.0 319.7 jit_solution(2802235716862108983)
XLA Ops:
  0.0 49.4 %shard_map.235.mix_ref = bf16[256,384]{1,0:T(8,128)(2,1)} custom-call(bf16[256,512]{1,0:T(8,128)(2,1)} %latent_hbm.1, bf16[64,256]{1,0:T(8,128)(2,1)} %bitcast.9, bf16[256,384]{1,0:T(8,128)(2,1)} %wide_query_hbm.1, bf16[256,256]{1,0:T(8,128)(2,1)} %narrow_query_hbm.1, bf16[512,256]{1,0:T(8,128)(2,1)} %wide_key_hbm.1, bf16[512,256]{1,0:T(8,128)(2,1)} %wide_value_hbm.1, ...), custom_call_target="tpu_custom_call" | custom-call | tf_op jit(solution)/shard_map/pallas_call | solution.py:348
  49.4 268.4 %shard_map.236 = bf16[64,4096]{1,0:T(8,128)(2,1)} custom-call(bf16[256,384]{1,0:T(8,128)(2,1)} %shard_map.235.mix_ref, s32[2,64]{1,0:T(2,128)} %bitcast.12, f32[2,64]{1,0:T(2,128)} %bitcast.13, bf16[256,4096]{1,0:T(8,128)(2,1)} %out_wide_hbm.1, bf16[128,4096]{1,0:T(8,128)(2,1)} %out_narrow_hbm.1, bf16[64,4096]{1,0:T(8,128)(2,1)} %residual_hbm.1, ...), custom_call_target="tpu_custom_call" | custom-call | tf_op jit(solution)/shard_map/pallas_call | solution.py:794
  317.8 1.9 copy.27

commit v5 on v3

--- a/solution.py
+++ b/solution.py
@@ -76,6 +76,7 @@
     x_recv,
     d_send,
     d_recv,
+    wrap_open,
 ):
     tokens, width = latent_hbm.shape
     quarter = tokens // n_tp
@@ -116,8 +117,15 @@
         copy.start()
 
     barrier = pltpu.get_barrier_semaphore()
-    for place in ({"sp": up * 2 + core}, {"sp": down * 2 + core}, {"sp": partner}, {"tp": left}, {"tp": right}):
+    for place in ({"sp": down * 2 + core}, {"sp": partner}, {"tp": left}, {"tp": right}):
         pl.semaphore_signal(barrier, inc=1, device_id=place, device_id_type=pl.DeviceIdType.MESH)
+
+    above = {"sp": up * 2 + core}
+
+    @pl.when(z < zn - 1)
+    def _():
+        pl.semaphore_signal(barrier, inc=1, device_id=above, device_id_type=pl.DeviceIdType.MESH)
+
 
     for copy in fetches:
         copy.wait()
@@ -157,7 +165,18 @@
     queries[3, :, LANES:] = turn(pltpu.roll(n1, half, 1))
     top[...] = jnp.full(top.shape, NEG_FILL, jnp.float32)
     mixed[...] = jnp.zeros(mixed.shape, jnp.float32)
-    pl.semaphore_wait(barrier, 5)
+
+    @pl.when(z > 0)
+    def _():
+        pl.semaphore_wait(barrier, 5)
+
+    @pl.when(z == 0)
+    def _():
+        pl.semaphore_wait(barrier, 4)
+
+    @pl.when(z == zn - 1)
+    def _():
+        pl.semaphore_signal(wrap_open, inc=1, device_id=above, device_id_type=pl.DeviceIdType.MESH)
 
     def along_z(d, k, j):
         block = jnp.where(d == 0, z - k + zn, z + k) % zn
@@ -257,7 +276,7 @@
     to_partner(0, 0).start()
     for d in range(2):
 
-        @pl.when(goes_on(d, 0))
+        @pl.when(goes_on(d, 0) & ((d == 0) | (z > 0)))
         def _():
             for j in range(2):
                 along_z(d, 0, j).start()
@@ -265,6 +284,12 @@
     to_partner(0, 0).wait_recv()
 
     attend(z, True)
+
+    @pl.when(z == 0)
+    def _():
+        pl.semaphore_wait(wrap_open, 1)
+        for j in range(2):
+            along_z(1, 0, j).start()
 
     def one_step(k, carry):
         def forward(d, c):
@@ -378,6 +403,7 @@
             dma((2, hops, 2)),
             dma((2, hops)),
             dma((2, hops)),
+            pltpu.SemaphoreType.REGULAR,
         ],
         compiler_params=pltpu.CompilerParams(
             collective_id=0, has_side_effects=True, vmem_limit_bytes=VMEM_BYTES
@@ -399,7 +425,7 @@
     )
 
 
-DELTAS = ((0, 1, -1, 4, -4, 5, -5, 8), (2, -2, 3, -3, 6, -6, 7, -7))
+DELTAS = ((0, 8, 7, -7, 4, -4, 1, -1), (6, -6, 5, -5, 3, -3, 2, -2))
 COLUMNS = 1024
 CAPACITY = 2
 
@@ -528,33 +554,88 @@
     for copy in fetches:
         copy.start()
 
+    def normed(values):
+        return rms_scale(values.astype(jnp.float32), gain_ref[...]).astype(jnp.bfloat16)
+
     def chunks():
         return [pl.ds(n, COLUMNS) for n in range(0, depth, COLUMNS)]
 
-    def project(dx):
+    half_cols = (pl.ds(0, half), pl.ds(half, half))
+    lower, upper = half_cols
+    split = half // 2
+
+    def sides(g):
+        return pl.ds(g * half, split), pl.ds(g * half + split, split)
+
+    def project(dx, g):
         q = pl.multiple_of(lax.rem(x + dx, n_tp) * rows, rows)
         mine = mix_ref[pl.ds(q, rows), :]
-        for cols in chunks():
+        for cols in sides(g):
             part[dx, :, cols] = jnp.dot(
                 mine, out_weight[:, cols], preferred_element_type=jnp.float32
             ).astype(jnp.bfloat16)
 
-    lower, upper = pl.ds(0, half), pl.ds(half, half)
+    sent = []
+
+    def begin(source, target, place):
+        copy = remote(source, target, place)
+        copy.start()
+        sent.append(copy)
+        return copy
+
+    def to_opposite(g):
+        left_side, right_side = sides(g)
+        return (
+            begin(part.at[2, :, left_side], opposite.at[g, 0], along_x(1)),
+            begin(part.at[2, :, right_side], opposite.at[g, 1], along_x(-1)),
+        )
+
+    def straight(g):
+        left_side, right_side = sides(g)
+        return (
+            begin(part.at[1, :, right_side], landed.at[g, 0, 1], along_x(1)),
+            begin(part.at[3, :, left_side], landed.at[g, 1, 0], along_x(-1)),
+        )
+
+    def joined(g, waiting):
+        copies = []
+        for side, (dx, cols) in enumerate(zip((1, 3), sides(g))):
+            waiting[side].wait_recv()
+            summed[g, side] = (
+                part[dx, :, cols].astype(jnp.float32) + opposite[g, side].astype(jnp.float32)
+            ).astype(jnp.bfloat16)
+            copies.append(
+                begin(summed.at[g, side], landed.at[g, side, side], along_x(1 if side == 0 else -1))
+            )
+        return tuple(copies)
+
+    def add_up(g, waiting):
+        for copy in waiting:
+            copy.wait_recv()
+        for side, cols in enumerate(sides(g)):
+            stream[:, cols] = (
+                residual_ref[:, cols].astype(jnp.float32)
+                + part[0, :, cols].astype(jnp.float32)
+                + landed[g, 0, side].astype(jnp.float32)
+                + landed[g, 1, side].astype(jnp.float32)
+            ).astype(jnp.bfloat16)
+        gathered[0, :, half_cols[g]] = stream[:, half_cols[g]]
+        for cols in sides(g):
+            outgoing[:, :, cols] = (
+                jnp.dot(send_map, gathered[0, :, cols], preferred_element_type=jnp.float32)
+                .astype(jnp.bfloat16)
+                .reshape(zn, piece, split)
+            )
+
     for copy in fetches[:4]:
         copy.wait()
-    project(2)
+    project(2, 0)
     pl.semaphore_wait(barrier, len(greeted))
-    over_right = remote(part.at[2, :, lower], opposite.at[0], along_x(1))
-    over_left = remote(part.at[2, :, upper], opposite.at[1], along_x(-1))
-    over_right.start()
-    over_left.start()
-    project(1)
-    straight_right = remote(part.at[1, :, upper], landed.at[0, 1], along_x(1))
-    straight_right.start()
-    project(3)
-    straight_left = remote(part.at[3, :, lower], landed.at[1, 0], along_x(-1))
-    straight_left.start()
-    project(0)
+    opposite_copies = [to_opposite(0)]
+    project(1, 0)
+    project(3, 0)
+    straight_copies = [straight(0)]
+    project(0, 0)
 
     r0 = lax.broadcasted_iota(jnp.int32, (rows, rows), 0)
     r1 = lax.broadcasted_iota(jnp.int32, (rows, rows), 1)
@@ -575,78 +656,39 @@
         places[c] = maps[c].T.astype(jnp.bfloat16)
     send_map = sum(maps[1:], maps[0]).astype(jnp.bfloat16)
 
-    over_right.wait_recv()
-    summed[0] = (part[1, :, lower].astype(jnp.float32) + opposite[0].astype(jnp.float32)).astype(jnp.bfloat16)
-    joined_right = remote(summed.at[0], landed.at[0, 0], along_x(1))
-    joined_right.start()
-    over_left.wait_recv()
-    summed[1] = (part[3, :, upper].astype(jnp.float32) + opposite[1].astype(jnp.float32)).astype(jnp.bfloat16)
-    joined_left = remote(summed.at[1], landed.at[1, 1], along_x(-1))
-    joined_left.start()
-    fetches[4].wait()
-    fetches[5].wait()
-    for copy in (straight_right, straight_left, joined_right, joined_left):
-        copy.wait_recv()
-    for h, cols in enumerate((lower, upper)):
-        stream[:, cols] = (
-            residual_ref[:, cols].astype(jnp.float32)
-            + part[0, :, cols].astype(jnp.float32)
-            + landed[0, h].astype(jnp.float32)
-            + landed[1, h].astype(jnp.float32)
-        ).astype(jnp.bfloat16)
-    gathered[0] = rms_scale(stream[...].astype(jnp.float32), gain_ref[...]).astype(jnp.bfloat16)
-
-    for cols in chunks():
-        outgoing[:, :, cols] = (
-            jnp.dot(send_map, gathered[0, :, cols], preferred_element_type=jnp.float32)
-            .astype(jnp.bfloat16)
-            .reshape(zn, piece, COLUMNS)
-        )
-    sent = [over_right, over_left, straight_right, straight_left, joined_right, joined_left]
+    project(2, 1)
+    joined_copies = [joined(0, opposite_copies[0])]
+    opposite_copies.append(to_opposite(1))
+    project(1, 1)
+    project(3, 1)
+    straight_copies.append(straight(1))
+    project(0, 1)
+    for copy in fetches[4:6]:
+        copy.wait()
+
     far = at_plane(8)
-    relay_up = remote(outgoing.at[far, :, lower], first_relay.at[0], on_plane(4))
-    relay_down = remote(outgoing.at[far, :, upper], first_relay.at[1], on_plane(-4))
-    relay_up.start()
-    relay_down.start()
-    first = [{}, {}]
-    for ch in range(2):
-        for j, delta in enumerate(DELTAS[ch]):
-            if delta in (0, 8):
-                continue
-            first[ch][j] = remote(outgoing.at[at_plane(delta)], first_recv.at[ch, j], on_plane(delta))
-            first[ch][j].start()
-        if ch == 0:
-            spread = [remote(gathered.at[0], gathered.at[dx], along_x(dx)) for dx in (1, 3, 2)]
-            for copy in spread:
-                copy.start()
+    first = [[], []]
+    relays_in = []
+    for g, cols in enumerate(half_cols):
+        add_up(g, straight_copies[g] + joined_copies[g])
+        relays_in.append(begin(outgoing.at[far, :, cols], first_relay.at[g], on_plane(4 if g == 0 else -4)))
+        for j, delta in enumerate(DELTAS[0]):
+            if delta not in (0, 8):
+                first[0].append(
+                    begin(outgoing.at[at_plane(delta), :, cols], first_recv.at[0, j, :, cols], on_plane(delta))
+                )
+        if g == 0:
+            joined_copies.append(joined(1, opposite_copies[1]))
+    for j, delta in enumerate(DELTAS[1]):
+        first[1].append(begin(outgoing.at[at_plane(delta)], first_recv.at[1, j], on_plane(delta)))
+    spread = [begin(gathered.at[0], gathered.at[dx], along_x(dx)) for dx in (1, 3, 2)]
     first_recv[0, 0] = outgoing[z]
     far_slot = DELTAS[0].index(8)
-    onward_up = remote(first_relay.at[0], first_recv.at[0, far_slot, :, lower], on_plane(4))
-    onward_down = remote(first_relay.at[1], first_recv.at[0, far_slot, :, upper], on_plane(-4))
-    relay_up.wait_recv()
-    onward_up.start()
-    relay_down.wait_recv()
-    onward_down.start()
-    sent += [relay_up, relay_down, onward_up, onward_down] + spread
-    sent += list(first[0].values()) + list(first[1].values())
-
-    for copy in fetches[6:]:
-        copy.wait()
-    for copy in spread:
-        copy.wait_recv()
-    every = gathered[...].reshape(n_tp * rows, depth)
-    both = jnp.dot(every, shared_in[...], preferred_element_type=jnp.float32)
-    act = (silu(both[:, :ff]) * both[:, ff:]).astype(jnp.bfloat16)
-    for cols in chunks():
-        shared_send[:, :, cols] = (
-            jnp.dot(act, shared_down[:, cols], preferred_element_type=jnp.float32)
-            .astype(jnp.bfloat16)
-            .reshape(n_tp, rows, COLUMNS)
-        )
-    shared_back = [remote(shared_send.at[dx], shared_recv.at[dx - 1], along_x(-dx)) for dx in range(1, n_tp)]
-    for copy in shared_back:
-        copy.start()
-    sent += shared_back
+    for g, cols in enumerate(half_cols):
+        relays_in[g].wait_recv()
+        first[0].append(
+            begin(first_relay.at[g], first_recv.at[0, far_slot, :, cols], on_plane(4 if g == 0 else -4))
+        )
 
     count = lanes * piece
     o = lax.broadcasted_iota(jnp.int32, (count, count), 0)
@@ -678,7 +720,7 @@
         return copies
 
     def run_expert(ch):
-        taken_in = second_recv[ch].reshape(count, depth)
+        taken_in = normed(second_recv[ch].reshape(count, depth))
         gate, lifted = (
             lax.dot_general(
                 taken_in,
@@ -724,9 +766,24 @@
                 copies[-1].start()
         return copies, relays
 
-    for copy in list(first[0].values()) + [onward_up, onward_down]:
+    for copy in first[0]:
         copy.wait_recv()
     lane_copies = to_lanes(0)
+
+    for copy in fetches[6:]:
+        copy.wait()
+    for copy in spread:
+        copy.wait_recv()
+    every = normed(gathered[...].reshape(n_tp * rows, depth))
+    both = jnp.dot(every, shared_in[...], preferred_element_type=jnp.float32)
+    act = (silu(both[:, :ff]) * both[:, ff:]).astype(jnp.bfloat16)
+    for cols in chunks():
+        shared_send[:, :, cols] = (
+            jnp.dot(act, shared_down[:, cols], preferred_element_type=jnp.float32)
+            .astype(jnp.bfloat16)
+            .reshape(n_tp, rows, COLUMNS)
+        )
+
     for copy in lane_copies:
         copy.wait_recv()
     back_copies = run_expert(0)
@@ -735,7 +792,7 @@
     home_copies, relays = home(0)
     sent += lane_copies + back_copies + home_copies + relays
 
-    for copy in first[1].values():
+    for copy in first[1]:
         copy.wait_recv()
     lane_copies = to_lanes(1)
     relays[0].wait_recv()
@@ -747,6 +804,10 @@
     for copy in lane_copies:
         copy.wait_recv()
     back_copies = run_expert(1)
+    shared_back = [remote(shared_send.at[dx], shared_recv.at[dx - 1], along_x(-dx)) for dx in range(1, n_tp)]
+    for copy in shared_back:
+        copy.start()
+    sent += shared_back
     for copy in back_copies:
         copy.wait_recv()
     more_home, _ = home(1)
@@ -811,9 +872,9 @@
             pltpu.VMEM((2 * hidden, depth), bf16),
             pltpu.VMEM(expert_down.shape[1:], bf16),
             pltpu.VMEM((n_tp, rows, depth), bf16),
-            pltpu.VMEM((2, rows, depth // 2), bf16),
-            pltpu.VMEM((2, rows, depth // 2), bf16),
-            pltpu.VMEM((2, 2, rows, depth // 2), bf16),
+            pltpu.VMEM((2, 2, rows, depth // 4), bf16),
+            pltpu.VMEM((2, 2, rows, depth // 4), bf16),
+            pltpu.VMEM((2, 2, 2, rows, depth // 4), bf16),
             pltpu.VMEM((rows, depth), bf16),
             pltpu.VMEM((n_tp, rows, depth), bf16),
             pltpu.VMEM((zn, piece, depth), bf16),
@@ -829,8 +890,8 @@
             pltpu.VMEM((n_tp, rows, depth), bf16),
             pltpu.VMEM((n_tp - 1, rows, depth), bf16),
             dma((12,)),
-            dma((80,)),
-            dma((80,)),
+            dma((104,)),
+            dma((104,)),
         ],
         compiler_params=pltpu.CompilerParams(
             collective_id=1, has_side_effects=True, vmem_limit_bytes=VMEM_BYTES

time: 320 us -> 308 us (0.963)
  Pallas kernels: 318 us -> 304 us
    pallas_call x1, Pallas kernels: 265 us -> 255 us  [projected_experts(): pl.pallas_call(functools.partial(experts_kernel, n_sp, n_tp), out_shape=j...]
    pallas_call x1, Pallas kernels: 52.8 us -> 49.4 us  [attention(): pl.pallas_call(functools.partial(attention_kernel, n_sp, n_tp), out_shape...]
where the time goes in v5:
time: 308 us; the launch traced here: 306 us
  Pallas kernels  304 us (99%)
    pallas_call x1, Pallas kernels, projected_experts(): pl.pallas_call(functools.partial(experts_kernel, n_sp, n_tp), out_shape=j...  255 us
    pallas_call x1, Pallas kernels, attention(): pl.pallas_call(functools.partial(attention_kernel, n_sp, n_tp), out_shape...  49.4 us

profile of v5, /device:TPU:35, one launch (start us, length us, event | category | flops | bytes accessed | tf_op | source)
XLA Modules:
  0.0 306.1 jit_solution(17731799197521542617)
XLA Ops:
  0.0 49.4 %shard_map.235.mix_ref = bf16[256,384]{1,0:T(8,128)(2,1)} custom-call(bf16[256,512]{1,0:T(8,128)(2,1)} %latent_hbm.1, bf16[64,256]{1,0:T(8,128)(2,1)} %bitcast.9, bf16[256,384]{1,0:T(8,128)(2,1)} %wide_query_hbm.1, bf16[256,256]{1,0:T(8,128)(2,1)} %narrow_query_hbm.1, bf16[512,256]{1,0:T(8,128)(2,1)} %wide_key_hbm.1, bf16[512,256]{1,0:T(8,128)(2,1)} %wide_value_hbm.1, ...), custom_call_target="tpu_custom_call" | custom-call | tf_op jit(solution)/shard_map/pallas_call | solution.py:377
  49.4 254.9 %shard_map.236 = bf16[64,4096]{1,0:T(8,128)(2,1)} custom-call(bf16[256,384]{1,0:T(8,128)(2,1)} %shard_map.235.mix_ref, s32[2,64]{1,0:T(2,128)} %bitcast.12, f32[2,64]{1,0:T(2,128)} %bitcast.13, bf16[256,4096]{1,0:T(8,128)(2,1)} %out_wide_hbm.1, bf16[128,4096]{1,0:T(8,128)(2,1)} %out_narrow_hbm.1, bf16[64,4096]{1,0:T(8,128)(2,1)} %residual_hbm.1, ...), custom_call_target="tpu_custom_call" | custom-call | tf_op jit(solution)/shard_map/pallas_call | solution.py:858
  304.3 1.9 copy.27

commit v6 on v5

--- a/solution.py
+++ b/solution.py
@@ -201,7 +201,7 @@
             dst_ref=spot,
             send_sem=x_send.at[d, k, j],
             recv_sem=x_recv.at[d, k, j],
-            device_id={"tp": right if j == 0 else left},
+            device_id={"tp": jnp.where(j == 0, right, left)},
             device_id_type=pl.DeviceIdType.MESH,
         )
 
@@ -292,44 +292,44 @@
             along_z(1, 0, j).start()
 
     def one_step(k, carry):
-        def forward(d, c):
-            @pl.when(arrives(d, k))
+        def quarter_step(j, carry):
+            def forward(d, c):
+                @pl.when(arrives(d, k))
+                def _():
+                    along_z(d, k - 1, j).wait_recv()
+
+                @pl.when(goes_on(d, k))
+                def _():
+                    along_z(d, k, j).start()
+
+                @pl.when(seen(d, k))
+                def _():
+                    along_x(d, k, j).start()
+
+                return c
+
+            def share(d, c):
+                @pl.when(seen(d, k - 1) & (j == 1))
+                def _():
+                    for side in range(2):
+                        along_x(d, k - 1, side).wait_recv()
+                    to_partner(d, k - 1).start()
+
+                return c
+
+            lax.fori_loop(0, 2, forward, 0)
+            lax.fori_loop(0, 2, share, 0)
+
+            @pl.when(seen(j, k - 3))
             def _():
-                for j in range(2):
-                    along_z(d, k - 1, j).wait_recv()
-
-            @pl.when(goes_on(d, k))
-            def _():
-                for j in range(2):
-                    along_z(d, k, j).start()
-
-            @pl.when(seen(d, k))
-            def _():
-                for j in range(2):
-                    along_x(d, k, j).start()
-
-            @pl.when(seen(d, k - 1))
-            def _():
-                for j in range(2):
-                    along_x(d, k - 1, j).wait_recv()
-                to_partner(d, k - 1).start()
-
-            return c
-
-        lax.fori_loop(0, 2, forward, 0)
-
-        def work(d, c):
-            @pl.when(seen(d, k - 2))
-            def _():
-                to_partner(d, k - 2).wait_recv()
-                attend(jnp.where(d == 0, z - k + 2, z + k - 2 - zn), False)
-
-            return c
-
-        lax.fori_loop(0, 2, work, 0)
-        return carry
-
-    lax.fori_loop(1, steps_up + 3, one_step, 0)
+                to_partner(j, k - 3).wait_recv()
+                attend(jnp.where(j == 0, z - k + 3, z + k - 3 - zn), False)
+
+            return carry
+
+        return lax.fori_loop(0, 2, quarter_step, carry)
+
+    lax.fori_loop(1, steps_up + 4, one_step, 0)
 
     to_partner(0, 0).wait_send()
 

time: 308 us -> 301 us (0.977)
  Pallas kernels: 304 us -> 299 us
    pallas_call x1, Pallas kernels: 255 us -> 249 us  [projected_experts(): pl.pallas_call(functools.partial(experts_kernel, n_sp, n_tp), out_shape=j...]
where the time goes in v6:
time: 301 us
  Pallas kernels  299 us (99%)
    pallas_call x1, Pallas kernels, projected_experts(): pl.pallas_call(functools.partial(experts_kernel, n_sp, n_tp), out_shape=j...  249 us
    pallas_call x1, Pallas kernels, attention(): pl.pallas_call(functools.partial(attention_kernel, n_sp, n_tp), out_shape...  50.8 us

profile of v6, /device:TPU:35, one launch (start us, length us, event | category | flops | bytes accessed | tf_op | source)
XLA Modules:
  0.0 301.2 jit_solution(13533609501610417644)
XLA Ops:
  0.0 50.8 %shard_map.235.mix_ref = bf16[256,384]{1,0:T(8,128)(2,1)} custom-call(bf16[256,512]{1,0:T(8,128)(2,1)} %latent_hbm.1, bf16[64,256]{1,0:T(8,128)(2,1)} %bitcast.9, bf16[256,384]{1,0:T(8,128)(2,1)} %wide_query_hbm.1, bf16[256,256]{1,0:T(8,128)(2,1)} %narrow_query_hbm.1, bf16[512,256]{1,0:T(8,128)(2,1)} %wide_key_hbm.1, bf16[512,256]{1,0:T(8,128)(2,1)} %wide_value_hbm.1, ...), custom_call_target="tpu_custom_call" | custom-call | tf_op jit(solution)/shard_map/pallas_call | solution.py:377
  50.8 248.5 %shard_map.236 = bf16[64,4096]{1,0:T(8,128)(2,1)} custom-call(bf16[256,384]{1,0:T(8,128)(2,1)} %shard_map.235.mix_ref, s32[2,64]{1,0:T(2,128)} %bitcast.12, f32[2,64]{1,0:T(2,128)} %bitcast.13, bf16[256,4096]{1,0:T(8,128)(2,1)} %out_wide_hbm.1, bf16[128,4096]{1,0:T(8,128)(2,1)} %out_narrow_hbm.1, bf16[64,4096]{1,0:T(8,128)(2,1)} %residual_hbm.1, ...), custom_call_target="tpu_custom_call" | custom-call | tf_op jit(solution)/shard_map/pallas_call | solution.py:858
  299.4 1.9 copy.27

commit v7 on v6

--- a/solution.py
+++ b/solution.py
@@ -425,7 +425,7 @@
     )
 
 
-DELTAS = ((0, 8, 7, -7, 4, -4, 1, -1), (6, -6, 5, -5, 3, -3, 2, -2))
+DELTAS = ((0, 6, -6, 5, -5, 2, -2, 1), (8, 7, -7, 4, -4, 3, -3, -1))
 COLUMNS = 1024
 CAPACITY = 2
 
@@ -679,16 +679,17 @@
                 )
         if g == 0:
             joined_copies.append(joined(1, opposite_copies[1]))
-    for j, delta in enumerate(DELTAS[1]):
-        first[1].append(begin(outgoing.at[at_plane(delta)], first_recv.at[1, j], on_plane(delta)))
     spread = [begin(gathered.at[0], gathered.at[dx], along_x(dx)) for dx in (1, 3, 2)]
     first_recv[0, 0] = outgoing[z]
-    far_slot = DELTAS[0].index(8)
+    far_slot = DELTAS[1].index(8)
     for g, cols in enumerate(half_cols):
         relays_in[g].wait_recv()
-        first[0].append(
-            begin(first_relay.at[g], first_recv.at[0, far_slot, :, cols], on_plane(4 if g == 0 else -4))
-        )
+        first[1].append(
+            begin(first_relay.at[g], first_recv.at[1, far_slot, :, cols], on_plane(4 if g == 0 else -4))
+        )
+    for j, delta in enumerate(DELTAS[1]):
+        if delta != 8:
+            first[1].append(begin(outgoing.at[at_plane(delta)], first_recv.at[1, j], on_plane(delta)))
 
     count = lanes * piece
     o = lax.broadcasted_iota(jnp.int32, (count, count), 0)
@@ -789,18 +790,12 @@
     back_copies = run_expert(0)
     for copy in back_copies:
         copy.wait_recv()
-    home_copies, relays = home(0)
-    sent += lane_copies + back_copies + home_copies + relays
+    home_copies, _ = home(0)
+    sent += lane_copies + back_copies + home_copies
 
     for copy in first[1]:
         copy.wait_recv()
     lane_copies = to_lanes(1)
-    relays[0].wait_recv()
-    last_up = remote(back_relay.at[0], returned.at[at_plane(-4), :, lower], on_plane(4))
-    last_up.start()
-    relays[1].wait_recv()
-    last_down = remote(back_relay.at[1], returned.at[at_plane(4), :, upper], on_plane(-4))
-    last_down.start()
     for copy in lane_copies:
         copy.wait_recv()
     back_copies = run_expert(1)
@@ -810,8 +805,14 @@
     sent += shared_back
     for copy in back_copies:
         copy.wait_recv()
-    more_home, _ = home(1)
-    sent += lane_copies + back_copies + more_home + [last_up, last_down]
+    more_home, relays = home(1)
+    relays[0].wait_recv()
+    last_up = remote(back_relay.at[0], returned.at[at_plane(-4), :, lower], on_plane(4))
+    last_up.start()
+    relays[1].wait_recv()
+    last_down = remote(back_relay.at[1], returned.at[at_plane(4), :, upper], on_plane(-4))
+    last_down.start()
+    sent += lane_copies + back_copies + more_home + relays + [last_up, last_down]
 
     for copy in shared_back:
         copy.wait_recv()

time: 301 us -> 276 us (0.917)
  Pallas kernels: 299 us -> 273 us
    pallas_call x1, Pallas kernels: 249 us -> 222 us  [projected_experts(): pl.pallas_call(functools.partial(experts_kernel, n_sp, n_tp), out_shape=j...]
where the time goes in v7:
time: 276 us; the launch traced here: 275 us
  Pallas kernels  273 us (99%)
    pallas_call x1, Pallas kernels, projected_experts(): pl.pallas_call(functools.partial(experts_kernel, n_sp, n_tp), out_shape=j...  222 us
    pallas_call x1, Pallas kernels, attention(): pl.pallas_call(functools.partial(attention_kernel, n_sp, n_tp), out_shape...  50.8 us

profile of v7, /device:TPU:35, one launch (start us, length us, event | category | flops | bytes accessed | tf_op | source)
XLA Modules:
  0.0 274.6 jit_solution(15408708118943430298)
XLA Ops:
  0.0 50.8 %shard_map.235.mix_ref = bf16[256,384]{1,0:T(8,128)(2,1)} custom-call(bf16[256,512]{1,0:T(8,128)(2,1)} %latent_hbm.1, bf16[64,256]{1,0:T(8,128)(2,1)} %bitcast.9, bf16[256,384]{1,0:T(8,128)(2,1)} %wide_query_hbm.1, bf16[256,256]{1,0:T(8,128)(2,1)} %narrow_query_hbm.1, bf16[512,256]{1,0:T(8,128)(2,1)} %wide_key_hbm.1, bf16[512,256]{1,0:T(8,128)(2,1)} %wide_value_hbm.1, ...), custom_call_target="tpu_custom_call" | custom-call | tf_op jit(solution)/shard_map/pallas_call | solution.py:377
  50.8 221.9 %shard_map.236 = bf16[64,4096]{1,0:T(8,128)(2,1)} custom-call(bf16[256,384]{1,0:T(8,128)(2,1)} %shard_map.235.mix_ref, s32[2,64]{1,0:T(2,128)} %bitcast.12, f32[2,64]{1,0:T(2,128)} %bitcast.13, bf16[256,4096]{1,0:T(8,128)(2,1)} %out_wide_hbm.1, bf16[128,4096]{1,0:T(8,128)(2,1)} %out_narrow_hbm.1, bf16[64,4096]{1,0:T(8,128)(2,1)} %residual_hbm.1, ...), custom_call_target="tpu_custom_call" | custom-call | tf_op jit(solution)/shard_map/pallas_call | solution.py:859
  272.7 1.9 copy.27

commit v8 on v7

--- a/solution.py
+++ b/solution.py
@@ -551,7 +551,7 @@
             )
         )
     ]
-    for copy in fetches:
+    for copy in fetches[:6]:
         copy.start()
 
     def normed(values):
@@ -629,6 +629,8 @@
 
     for copy in fetches[:4]:
         copy.wait()
+    for copy in fetches[6:]:
+        copy.start()
     project(2, 0)
     pl.semaphore_wait(barrier, len(greeted))
     opposite_copies = [to_opposite(0)]
@@ -656,8 +658,8 @@
         places[c] = maps[c].T.astype(jnp.bfloat16)
     send_map = sum(maps[1:], maps[0]).astype(jnp.bfloat16)
 
+    joined_copies = [joined(0, opposite_copies[0])]
     project(2, 1)
-    joined_copies = [joined(0, opposite_copies[0])]
     opposite_copies.append(to_opposite(1))
     project(1, 1)
     project(3, 1)

time: 276 us -> 276 us (level)
  no operation moved by 1% of the time
where the time goes in v8:
time: 276 us; the launch traced here: 275 us
  Pallas kernels  273 us (99%)
    pallas_call x1, Pallas kernels, projected_experts(): pl.pallas_call(functools.partial(experts_kernel, n_sp, n_tp), out_shape=j...  222 us
    pallas_call x1, Pallas kernels, attention(): pl.pallas_call(functools.partial(attention_kernel, n_sp, n_tp), out_shape...  50.8 us

profile of v8, /device:TPU:35, one launch (start us, length us, event | category | flops | bytes accessed | tf_op | source)
XLA Modules:
  0.0 274.6 jit_solution(6173481210855185765)
XLA Ops:
  0.0 50.8 %shard_map.235.mix_ref = bf16[256,384]{1,0:T(8,128)(2,1)} custom-call(bf16[256,512]{1,0:T(8,128)(2,1)} %latent_hbm.1, bf16[64,256]{1,0:T(8,128)(2,1)} %bitcast.9, bf16[256,384]{1,0:T(8,128)(2,1)} %wide_query_hbm.1, bf16[256,256]{1,0:T(8,128)(2,1)} %narrow_query_hbm.1, bf16[512,256]{1,0:T(8,128)(2,1)} %wide_key_hbm.1, bf16[512,256]{1,0:T(8,128)(2,1)} %wide_value_hbm.1, ...), custom_call_target="tpu_custom_call" | custom-call | tf_op jit(solution)/shard_map/pallas_call | solution.py:377
  50.8 221.9 %shard_map.236 = bf16[64,4096]{1,0:T(8,128)(2,1)} custom-call(bf16[256,384]{1,0:T(8,128)(2,1)} %shard_map.235.mix_ref, s32[2,64]{1,0:T(2,128)} %bitcast.12, f32[2,64]{1,0:T(2,128)} %bitcast.13, bf16[256,4096]{1,0:T(8,128)(2,1)} %out_wide_hbm.1, bf16[128,4096]{1,0:T(8,128)(2,1)} %out_narrow_hbm.1, bf16[64,4096]{1,0:T(8,128)(2,1)} %residual_hbm.1, ...), custom_call_target="tpu_custom_call" | custom-call | tf_op jit(solution)/shard_map/pallas_call | solution.py:861
  272.8 1.9 copy.27

commit v9 on v8

--- a/solution.py
+++ b/solution.py
@@ -425,7 +425,7 @@
     )
 
 
-DELTAS = ((0, 6, -6, 5, -5, 2, -2, 1), (8, 7, -7, 4, -4, 3, -3, -1))
+DELTAS = ((0, 6, -6, 5, -5, 3, -3, 1), (8, 7, -7, 4, -4, 2, -2, -1))
 COLUMNS = 1024
 CAPACITY = 2
 

time: 276 us -> 276 us (level)
  no operation moved by 1% of the time
where the time goes in v9:
time: 276 us; the launch traced here: 274 us
  Pallas kernels  272 us (99%)
    pallas_call x1, Pallas kernels, projected_experts(): pl.pallas_call(functools.partial(experts_kernel, n_sp, n_tp), out_shape=j...  221 us
    pallas_call x1, Pallas kernels, attention(): pl.pallas_call(functools.partial(attention_kernel, n_sp, n_tp), out_shape...  50.8 us

profile of v9, /device:TPU:35, one launch (start us, length us, event | category | flops | bytes accessed | tf_op | source)
XLA Modules:
  0.0 273.8 jit_solution(1624758726225404945)
XLA Ops:
  0.0 50.8 %shard_map.235.mix_ref = bf16[256,384]{1,0:T(8,128)(2,1)} custom-call(bf16[256,512]{1,0:T(8,128)(2,1)} %latent_hbm.1, bf16[64,256]{1,0:T(8,128)(2,1)} %bitcast.9, bf16[256,384]{1,0:T(8,128)(2,1)} %wide_query_hbm.1, bf16[256,256]{1,0:T(8,128)(2,1)} %narrow_query_hbm.1, bf16[512,256]{1,0:T(8,128)(2,1)} %wide_key_hbm.1, bf16[512,256]{1,0:T(8,128)(2,1)} %wide_value_hbm.1, ...), custom_call_target="tpu_custom_call" | custom-call | tf_op jit(solution)/shard_map/pallas_call | solution.py:377
  50.8 221.0 %shard_map.236 = bf16[64,4096]{1,0:T(8,128)(2,1)} custom-call(bf16[256,384]{1,0:T(8,128)(2,1)} %shard_map.235.mix_ref, s32[2,64]{1,0:T(2,128)} %bitcast.12, f32[2,64]{1,0:T(2,128)} %bitcast.13, bf16[256,4096]{1,0:T(8,128)(2,1)} %out_wide_hbm.1, bf16[128,4096]{1,0:T(8,128)(2,1)} %out_narrow_hbm.1, bf16[64,4096]{1,0:T(8,128)(2,1)} %residual_hbm.1, ...), custom_call_target="tpu_custom_call" | custom-call | tf_op jit(solution)/shard_map/pallas_call | solution.py:861
  271.9 1.9 copy.27
